TPU v7x, 32 devices: a whole 2x2x4 slice. The times are simulated.
32 devices in a mesh: sp: 4 (over z), tp: 4 (over y, x), dp: 2 (over core).
Axes of the slice: x: 2, y: 2, z: 4, core: 2. Of those that a mesh axis runs over, the one named last changes fastest.
Arguments:
- latent: bfloat16 [2048, 2048], P(('dp', 'sp', 'tp')), parts along dimension 0, may hold values from -6 to 6
- context: bfloat16 [512, 2048], P(('dp', 'sp')), parts along dimension 0, may hold values from -6 to 6
- cond: bfloat16 [4096], P(('dp', 'sp')), parts along dimension 0, may hold values from -6 to 6
- context_cond: bfloat16 [2048], P('sp'), may hold values from -6 to 6
- norm_gain: float32 [2048], replicated, may hold values from 0.1 to 1.9
- mod_shift: bfloat16 [2048, 2048], P('sp', 'tp'), may hold values from -0.125 to 0.125
- mod_scale: bfloat16 [2048, 2048], P('sp', 'tp'), may hold values from -0.125 to 0.125
- mod_gate: bfloat16 [2048, 2048], P('sp', 'tp'), may hold values from -0.125 to 0.125
- w_query: bfloat16 [2048, 1024], P(None, 'tp'), may hold values from -0.125 to 0.125
- w_key: bfloat16 [2048, 1024], P(None, 'tp'), may hold values from -0.125 to 0.125
- w_value: bfloat16 [2048, 1024], P(None, 'tp'), may hold values from -0.125 to 0.125
- query_gain: float32 [64], replicated, may hold values from 1.4 to 2.2
- key_gain: float32 [64], replicated, may hold values from 0.1 to 1.9
- mix_lambda: float32 [8], P('tp'), may hold values from 0.3 to 0.8
- context_lift: float32 [8], P('tp'), may hold values from 1.5 to 2.5
- value_gain: float32 [128], replicated, may hold values from 0.1 to 1.9
- w_out: bfloat16 [1024, 2048], P('tp'), may hold values from -0.1875 to 0.1875
Outputs:
- output: bfloat16 [2048, 2048], P(('dp', 'sp', 'tp')), parts along dimension 0
There are 2 independent parts, one for each index of `dp`. A program takes and returns all parts, laid end to end along the dimension named above; an argument that names none is the same for every part. Nothing has to cross between parts.
All inputs are finite; a program needn't handle non-finite values.
Results may differ from a plain program's by a relative error of at most 0.006.
Values may be sent and summed in bfloat16 or wider, within the bound.
A program may use at most 64 MiB of HBM per device.

v0:
```python
import functools

import jax
import jax.numpy as jnp
import numpy as np
from jax import lax
from jax.experimental import pallas as pl
from jax.experimental.pallas import tpu as pltpu
from jax.sharding import PartitionSpec as P

GRID = 64
token_eps = 0.01
head_eps = 0.001
rope_base = 10000.0
head_factor = 0.8
MESH = pl.DeviceIdType.MESH
BF = jnp.bfloat16
F32 = jnp.float32


def rope_tables(length, width):
    quarter = width // 4
    inverse = (rope_base ** (-np.arange(quarter, dtype=np.float64) / quarter)).astype(np.float32)
    pos = np.arange(length)
    row = (pos // GRID).astype(np.float32)[:, None] * inverse
    col = (pos % GRID).astype(np.float32)[:, None] * inverse
    cos = np.concatenate([np.cos(row), np.cos(row), np.cos(col), np.cos(col)], axis=1)
    sin = np.concatenate([-np.sin(row), np.sin(row), -np.sin(col), np.sin(col)], axis=1)
    return np.tile(cos, (1, 2)).astype(np.float32), np.tile(sin, (1, 2)).astype(np.float32)


def kernel(n_sp, n_tp, n_dp, head_width, *refs):
    (
        lat_h, ctx_h, cond_h, cctx_h, gain_h, ms_h, msc_h, mg_h, wq_h, wk_h, wv_h,
        qg_h, kg_h, vg_h, lam_r, lift_r, wo_h, cos_h, sin_h,
        out_r,
        cond_r, cctx_r, gain_r, qg_r, kg_r, vg_r,
        lat, ctx, mw, wq, wk, wv, wo, cosv, sinv,
        act, part, mod_in, summed, mod_full, vecs, invs, normed, qown, qin, qm, kvl, kvr, acc, mine, ho,
        loc, bs_lat, br_lat, bs_mod, br_mod, bs_mt, br_mt, bs_kv, br_kv, bs_wo, br_wo,
        bs_dd, br_dd, bs_ho, br_ho, bs_q, br_q,
    ) = refs
    s = lax.axis_index("sp")
    t = lax.axis_index("tp")
    d_ix = lax.axis_index("dp")
    core = lax.rem(d_ix, 2)
    partner = d_ix + 1 - 2 * core
    t_odd = lax.rem(t, 2)
    nbr1 = t + 1 - 2 * t_odd
    nbr2 = lax.rem(t + 2, 4)
    nbr3 = lax.rem(nbr1 + 2, 4)
    peers = (t, nbr1, nbr2, nbr3)
    e = lax.rem(s, 2)
    pair = s + 1 - 2 * e
    R = lat.shape[1]
    HR = R // 2
    C = ctx.shape[0]
    D = lat.shape[2]
    QW = wq.shape[1]
    n_head = QW // (2 * head_width)
    HW = 2 * head_width
    VW = wv.shape[1] // n_head
    ROWS = 4 * R

    def local(i, src, dst):
        c = pltpu.make_async_copy(src, dst, loc.at[i])
        c.start()
        return c

    l_one = [
        local(11 + j, src, dst)
        for j, (src, dst) in enumerate(
            ((cond_h, cond_r), (cctx_h, cctx_r), (gain_h, gain_r), (qg_h, qg_r), (kg_h, kg_r),
             (vg_h, vg_r))
        )
    ]
    l_lat = local(0, lat_h, lat.at[0])
    l_mod = [local(1 + j, h, mw.at[j]) for j, h in enumerate((ms_h, msc_h, mg_h))]
    l_ctx = local(4, ctx_h, ctx)
    l_wk = local(5, wk_h, wk)
    l_wv = local(6, wv_h, wv)
    l_wq = local(7, wq_h, wq)
    l_wo = local(8, wo_h, wo.at[0])
    l_cos = local(9, cos_h.at[pl.ds(s * ROWS, ROWS)], cosv)
    l_sin = local(10, sin_h.at[pl.ds(s * ROWS, ROWS)], sinv)

    bar = pltpu.get_barrier_semaphore()
    for k in range(1, n_sp):
        pl.semaphore_signal(bar, inc=1, device_id={"sp": lax.rem(s + k, n_sp)}, device_id_type=MESH)
    for k in range(1, 4):
        pl.semaphore_signal(bar, inc=1, device_id={"tp": peers[k]}, device_id_type=MESH)
        pl.semaphore_signal(
            bar, inc=1, device_id={"sp": pair, "tp": peers[k]}, device_id_type=MESH
        )
    pl.semaphore_signal(bar, inc=1, device_id={"dp": partner}, device_id_type=MESH)

    act[...] = jnp.zeros_like(act)
    for row, ref in ((0, cond_r), (1, cctx_r)):
        l_one[row].wait()
        v = ref[...].astype(F32).reshape(1, -1)
        act[row : row + 1, :] = v / (1.0 + jnp.exp(-v))
    acts = act[...].astype(BF)
    part[...] = jnp.zeros_like(part)
    for j in range(3):
        l_mod[j].wait()
        res = jnp.dot(acts, mw[j], preferred_element_type=F32)
        part[2 * j : 2 * j + 2, :] = res[0:2]

    pl.semaphore_wait(bar, n_sp + 6)

    def remote(src, dst, ss, rs, where):
        return pltpu.make_async_remote_copy(
            src_ref=src, dst_ref=dst, send_sem=ss, recv_sem=rs, device_id=where, device_id_type=MESH
        )

    mod_copies = []
    for k in range(1, n_sp):
        c = remote(part, mod_in.at[k - 1], bs_mod.at[k - 1], br_mod.at[k - 1],
                   {"sp": lax.rem(s + k, n_sp)})
        c.start()
        mod_copies.append(c)

    l_lat.wait()

    def lat_copy(i, src_slot, dst_slot, half, where):
        rows = pl.ds(half * HR, HR)
        return remote(lat.at[src_slot, rows], lat.at[dst_slot, rows], bs_lat.at[i], br_lat.at[i],
                      {"tp": where})

    x0 = lat_copy(0, 0, 1, 0, nbr1)
    y1 = lat_copy(1, 0, 2, 1, nbr2)
    x1 = lat_copy(2, 0, 1, 1, nbr1)
    y0 = lat_copy(3, 0, 2, 0, nbr2)
    f0 = lat_copy(4, 1, 3, 0, nbr2)
    f1 = lat_copy(5, 2, 3, 1, nbr1)
    for c in (x0, y1):
        c.start()

    l_ctx.wait()

    def inverse_rows(src, count, dst_at):
        for i in range(count // 16):
            v = src[i * 16 : (i + 1) * 16, :].astype(F32)
            inv = lax.rsqrt(jnp.mean(v * v, axis=-1, keepdims=True) + token_eps)
            invs[dst_at + i * 16 : dst_at + (i + 1) * 16, :] = jnp.broadcast_to(inv, (16, 128))

    inverse_rows(ctx, C, 0)
    inverse_rows(lat.at[0], R, C)

    total = part[...]
    for k in range(n_sp - 1):
        mod_copies[k].wait_recv()
        total = total + mod_in[k]
    summed[...] = total
    mod_full[t] = total
    tp_copies = []
    for k in range(1, 4):
        c = remote(summed, mod_full.at[t], bs_mt.at[k - 1], br_mt.at[k - 1], {"tp": peers[k]})
        c.start()
        tp_copies.append(c)
    x1.start()
    y0.start()
    x0.wait_recv()
    f0.start()
    y1.wait_recv()
    f1.start()

    for k in range(1, 4):
        remote(summed, mod_full.at[peers[k]], bs_mt.at[k - 1], br_mt.at[k - 1],
               {"tp": peers[k]}).wait_recv()

    def full_row(j):
        return jnp.concatenate([mod_full[q, j : j + 1, :] for q in range(n_tp)], axis=1)

    for c in l_one[2:]:
        c.wait()
    gain = gain_r[...].reshape(1, -1)
    q_gain = qg_r[...].reshape(1, -1)
    q_gain = jnp.concatenate([q_gain, q_gain], axis=1)
    k_gain = kg_r[...].reshape(1, -1)
    k_gain = jnp.concatenate([k_gain, k_gain], axis=1)
    v_gain = vg_r[...].reshape(1, -1)
    vecs[0:1, :] = full_row(0)
    vecs[1:2, :] = full_row(1)
    vecs[2:3, :] = gain * (1.0 + full_row(2))
    vecs[3:4, :] = gain * (1.0 + full_row(3))
    vecs[4:5, :] = full_row(4)

    HALF = wo.shape[1] // 2
    QUART = HALF // 2

    def wo_rows(q):
        return pl.ds(pl.multiple_of(core * HALF + q * QUART, QUART), QUART)

    def wo_copy(i, src_slot, dst_slot, q, where):
        return remote(wo.at[src_slot, wo_rows(q)], wo.at[dst_slot, wo_rows(q)], bs_wo.at[i],
                      br_wo.at[i], {"tp": where})

    def dd_copy(k):
        rows = pl.ds(pl.multiple_of(core * HALF, HALF), HALF)
        return remote(wo.at[k, rows], wo.at[k, rows], bs_dd.at[k - 1], br_dd.at[k - 1],
                      {"dp": partner})

    def dd_recv(k):
        rows = pl.ds(pl.multiple_of((1 - core) * HALF, HALF), HALF)
        return remote(wo.at[k, rows], wo.at[k, rows], bs_dd.at[k - 1], br_dd.at[k - 1],
                      {"dp": partner})

    wx0 = wo_copy(0, 0, 1, 0, nbr1)
    wy1 = wo_copy(1, 0, 2, 1, nbr2)
    wx1 = wo_copy(2, 0, 1, 1, nbr1)
    wy0 = wo_copy(3, 0, 2, 0, nbr2)
    wf0 = wo_copy(4, 1, 3, 0, nbr2)
    wf1 = wo_copy(5, 2, 3, 1, nbr1)

    def norm_rows(src, row, count, dst_at):
        step = 16

        @pl.loop(0, count // step, unroll=True)
        def _(i):
            at = pl.multiple_of(i * step, step)
            v = src[pl.ds(at, step), :].astype(F32)
            inv = lax.rsqrt(jnp.mean(v * v, axis=-1, keepdims=True) + token_eps)
            normed[pl.ds(dst_at + at, step), :] = (
                v * inv * vecs[2 + row : 3 + row, :] + vecs[row : row + 1, :]
            ).astype(BF)

    def apply_rows(src, row, count, dst_at):
        for i in range(count // 16):
            v = src[i * 16 : (i + 1) * 16, :].astype(F32)
            at = slice(dst_at + i * 16, dst_at + (i + 1) * 16)
            normed[at, :] = (
                v * invs[at, 0:1] * vecs[2 + row : 3 + row, :] + vecs[row : row + 1, :]
            ).astype(BF)

    group = (
        lax.broadcasted_iota(jnp.int32, (QW, QW), 0) // head_width
        == lax.broadcasted_iota(jnp.int32, (QW, QW), 1) // head_width
    )
    group = jnp.where(group, 1.0 / head_width, 0.0).astype(F32)

    def head_norm(x):
        mean = jnp.dot(x * x, group, precision=lax.Precision.HIGHEST, preferred_element_type=F32)
        return x * lax.rsqrt(mean + token_eps)

    def turn(y, cos, sin):
        lane = lax.broadcasted_iota(jnp.int32, y.shape, 1)
        front = lax.rem(lane, head_width // 2) < head_width // 4
        other = jnp.where(
            front,
            pltpu.roll(y, HW - head_width // 4, axis=1),
            pltpu.roll(y, head_width // 4, axis=1),
        )
        return y * cos + other * sin

    def project_block(k, first):
        rows = pl.ds(first + C, R)
        x = normed[C + k * R : C + (k + 1) * R, :]
        at = pl.ds(pl.multiple_of(peers[k] * R, R), R)
        cos, sin = cosv[at, :], sinv[at, :]
        kk = head_norm(jnp.dot(x, wk[...], preferred_element_type=F32))
        for h in range(n_head):
            y = kk[:, h * HW : (h + 1) * HW] * k_gain
            kvl[h, rows, 0:HW] = turn(y, cos, sin).astype(BF)
        vv = jnp.dot(x, wv[...], preferred_element_type=F32).astype(BF)
        for h in range(n_head):
            kvl[h, rows, HW:] = vv[:, h * VW : (h + 1) * VW]

    def project_queries():
        x = normed[C:, :]
        qq = head_norm(jnp.dot(x, wq[...], preferred_element_type=F32))
        for k in range(4):
            at = pl.ds(pl.multiple_of(peers[k] * R, R), R)
            cos, sin = cosv[at, :], sinv[at, :]
            for h in range(n_head):
                y = qq[k * R : (k + 1) * R, h * HW : (h + 1) * HW] * q_gain
                qown[h, k * R : (k + 1) * R, :] = (
                    turn(y, cos, sin) * (head_width ** -0.5)
                ).astype(BF)

    def split_maps(q, at):
        lane = lax.broadcasted_iota(jnp.int32, q.shape, 1)
        for m in range(2):
            qm[m, at : at + ROWS, :] = jnp.where(lane // head_width == m, q, jnp.zeros_like(q))

    chunks = ((0, C + R), (C + R, 2 * R), (C + 3 * R, R))

    def kv_copy(direction, dist, c, src, origin, where):
        at, count = chunks[c]
        i = (direction * (n_sp - 1) + dist - 1) * len(chunks) + c
        return remote(src.at[pl.ds(at, count)], kvr.at[origin, pl.ds(at, count)], bs_kv.at[i],
                      br_kv.at[i], {"sp": where})

    def side(direction, dist, c, act_on):
        sign = 1 - 2 * direction
        hop = 1 if dist == 1 else 2
        origin = s - sign * (dist - hop)
        where = s + sign * hop
        ok = jnp.logical_and(
            jnp.logical_and(origin >= 0, origin < n_sp),
            jnp.logical_and(where >= 0, where < n_sp),
        )

        @pl.when(ok)
        def _():
            if dist == 1:
                src = kvl.at[1 - e]
            elif dist == 2:
                src = kvl.at[e]
            else:
                src = kvr.at[origin]
            act_on(kv_copy(direction, dist, c, src, origin, where))

    def start(copy):
        copy.start()

    def drain(copy):
        copy.wait_send()

    def send_own(c):
        for dist in (1, 2):
            if dist < n_sp:
                for direction in (0, 1):
                    side(direction, dist, c, start)

    apply_rows(ctx, 1, C, 0)
    apply_rows(lat.at[0], 0, R, C)
    l_wk.wait()
    l_wv.wait()
    l_cos.wait()
    l_sin.wait()
    x = normed[0:C, :]
    kk = head_norm(jnp.dot(x, wk[...], preferred_element_type=F32))
    vv = jnp.dot(x, wv[...], preferred_element_type=F32).astype(BF)
    for h in range(n_head):
        kvl[h, 0:C, 0:HW] = (kk[:, h * HW : (h + 1) * HW] * k_gain).astype(BF)
        kvl[h, 0:C, HW:] = vv[:, h * VW : (h + 1) * VW]
    project_block(0, 0)
    send_own(0)

    x1.wait_recv()
    y0.wait_recv()
    l_wo.wait()
    for c in (wx0, wy1, wx1, wy0):
        c.start()
    norm_rows(lat.at[1], 0, R, C + R)
    norm_rows(lat.at[2], 0, R, C + 2 * R)
    project_block(1, R)
    project_block(2, 2 * R)
    send_own(1)
    f0.wait_recv()
    f1.wait_recv()
    norm_rows(lat.at[3], 0, R, C + 3 * R)
    project_block(3, 3 * R)
    send_own(2)

    def arrive(dist, c):
        for direction in (0, 1):
            origin = s - dist if direction == 0 else s + dist
            here = origin >= 0 if direction == 0 else origin < n_sp

            @pl.when(here)
            def _():
                kv_copy(direction, dist, c, kvr.at[origin], origin, s).wait_recv()

            if dist + 2 < n_sp:
                side(direction, dist + 2, c, start)

    l_wq.wait()
    project_queries()
    q_copy = remote(qown.at[1 - e], qin, bs_q, br_q, {"sp": pair})
    q_copy.start()
    split_maps(qown[e], 0)
    arrive(1, 0)

    QB = 2 * R
    lift = lift_r[e]

    def attend(block, at, keys, start_row, count, first):
        k = block[at : at + keys, 0:HW]
        v = block[at : at + keys, HW:]
        vx = jnp.concatenate([v, jnp.ones_like(v)], axis=1)
        key = lax.broadcasted_iota(jnp.int32, (1, keys), 1)
        for m in range(2):
            for b in range(count // QB):
                rows = slice(start_row + b * QB, start_row + (b + 1) * QB)
                sc = lax.dot_general(
                    qm[m, rows, :], k, (((1,), (1,)), ((), ())), preferred_element_type=F32
                )
                if at < C:
                    sc = sc + jnp.where(key < C - at, lift, 0.0)
                p = jnp.exp(sc).astype(BF)
                add = jnp.dot(p, vx, preferred_element_type=F32)
                if first:
                    acc[m, rows, :] = add
                else:
                    acc[m, rows, :] += add

    def attend_arrived(dist, at, keys):
        @pl.when(s - dist >= 0)
        def _():
            attend(kvr.at[s - dist], at, keys, 0, 2 * ROWS, False)

        @pl.when(s + dist < n_sp)
        def _():
            attend(kvr.at[s + dist], at, keys, 0, 2 * ROWS, False)

    attend(kvl.at[e], 0, C + ROWS, 0, ROWS, True)
    for c in range(1, len(chunks)):
        arrive(1, c)
    wx0.wait_recv()
    wf0.start()
    wy1.wait_recv()
    wf1.start()
    q_copy.wait_recv()
    split_maps(qin[...], ROWS)
    attend(kvl.at[e], 0, C + ROWS, ROWS, ROWS, True)

    for dist in range(1, n_sp):
        last = dist == n_sp - 1
        if dist > 1:
            for c in range(len(chunks)):
                arrive(dist, c)
                if last:
                    attend_arrived(dist, *chunks[c])
        if not last:
            attend_arrived(dist, 0, C + ROWS)
        if dist == 2 or (last and n_sp == 2):
            wx1.wait_recv()
            dd_copy(1).start()
            wy0.wait_recv()
            dd_copy(2).start()

    def ho_copy(q, k):
        i = q * 4 + k
        where = {"tp": peers[k]} if q == 0 else {"sp": pair, "tp": peers[k]}
        if q == 1 and k == 0:
            where = {"sp": pair}
        return remote(mine.at[q, k], ho.at[q, k], bs_ho.at[i], br_ho.at[i], where)

    for q, k in ((1, 3), (1, 1), (1, 2), (0, 3), (1, 0), (0, 1), (0, 2), (0, 0)):
        rows = slice((4 * q + k) * R, (4 * q + k + 1) * R)
        a0 = acc[0, rows, :]
        a1 = acc[1, rows, :]
        mixed = a0[:, :VW] / a0[:, VW:] - lam_r[e] * (a1[:, :VW] / a1[:, VW:])
        inv = lax.rsqrt(jnp.mean(mixed * mixed, axis=-1, keepdims=True) + head_eps)
        mine[q, k, :, :] = (mixed * inv * v_gain * head_factor).astype(BF)
        if q or k:
            ho_copy(q, k).start()

    wf0.wait_recv()
    wf1.wait_recv()
    dd_copy(3).start()

    def head_rows(q):
        return pl.ds(pl.multiple_of((e if q == 0 else 1 - e) * VW, VW), VW)

    out = jnp.dot(mine[0, 0], wo[0, head_rows(0), :], preferred_element_type=F32)
    for q, k in ((0, 1), (0, 2), (1, 0), (0, 3), (1, 1), (1, 2), (1, 3)):
        if q == 0:
            dd_recv(k).wait_recv()
        ho_copy(q, k).wait_recv()
        out += jnp.dot(ho[q, k], wo[k, head_rows(q), :], preferred_element_type=F32)
    out_r[...] = vecs[4:5, :] * out

    for c in mod_copies + tp_copies + [x0, y1, x1, y0, f0, f1, wx0, wy1, wx1, wy0, wf0, wf1]:
        c.wait_send()
    for k in range(1, 4):
        dd_copy(k).wait_send()
    q_copy.wait_send()
    for q in range(2):
        for k in range(4):
            if q or k:
                ho_copy(q, k).wait_send()
    for dist in range(1, n_sp):
        for c in range(len(chunks)):
            for direction in (0, 1):
                side(direction, dist, c, drain)


def on_device(n_sp, n_tp, n_dp, *args):
    (
        latent, context, cond, context_cond, norm_gain, mod_shift, mod_scale, mod_gate,
        w_query, w_key, w_value, query_gain, key_gain, mix_lambda, context_lift, value_gain, w_out,
    ) = args
    R, D = latent.shape
    C = context.shape[0]
    head_width = query_gain.shape[0]
    cos, sin = rope_tables(R * n_sp * n_tp, head_width)
    QW, VWALL = w_query.shape[1], w_value.shape[1]
    heads = mix_lambda.shape[0]
    ROWS = R * n_tp
    MC = mod_shift.shape[1]
    chunk_sems = 2 * max(n_sp - 1, 1) * 3
    vm = pl.BlockSpec(memory_space=pltpu.VMEM)
    anywhere = pl.BlockSpec(memory_space=pl.ANY)
    smem = pl.BlockSpec(memory_space=pltpu.SMEM)
    dma = pltpu.SemaphoreType.DMA
    update = pl.pallas_call(
        functools.partial(kernel, n_sp, n_tp, n_dp, head_width),
        out_shape=pltpu.VMEM((R, D), F32),
        in_specs=[anywhere] * 14 + [smem, smem]
        + [anywhere] * 3,
        out_specs=vm,
        scratch_shapes=[
            pltpu.VMEM(cond.shape, BF),
            pltpu.VMEM(context_cond.shape, BF),
            pltpu.VMEM(norm_gain.shape, F32),
            pltpu.VMEM(query_gain.shape, F32),
            pltpu.VMEM(key_gain.shape, F32),
            pltpu.VMEM(value_gain.shape, F32),
            pltpu.VMEM((4, R, D), BF),
            pltpu.VMEM((C, D), BF),
            pltpu.VMEM((3,) + mod_shift.shape, BF),
            pltpu.VMEM(w_query.shape, BF),
            pltpu.VMEM(w_key.shape, BF),
            pltpu.VMEM(w_value.shape, BF),
            pltpu.VMEM((4,) + w_out.shape, BF),
            pltpu.VMEM((ROWS, 2 * head_width), F32),
            pltpu.VMEM((ROWS, 2 * head_width), F32),
            pltpu.VMEM((8, mod_shift.shape[0]), F32),
            pltpu.VMEM((8, MC), F32),
            pltpu.VMEM((max(n_sp - 1, 1), 8, MC), F32),
            pltpu.VMEM((8, MC), F32),
            pltpu.VMEM((n_tp, 8, MC), F32),
            pltpu.VMEM((8, D), F32),
            pltpu.VMEM((C + R, 128), F32),
            pltpu.VMEM((C + ROWS, D), BF),
            pltpu.VMEM((heads, ROWS, 2 * head_width), BF),
            pltpu.VMEM((ROWS, 2 * head_width), BF),
            pltpu.VMEM((2, 2 * ROWS, 2 * head_width), BF),
            pltpu.VMEM((heads, C + ROWS, (QW + VWALL) // heads), BF),
            pltpu.VMEM((n_sp, C + ROWS, (QW + VWALL) // heads), BF),
            pltpu.VMEM((2, 2 * ROWS, 2 * VWALL // heads), F32),
            pltpu.VMEM((2, 4, R, VWALL // heads), BF),
            pltpu.VMEM((2, 4, R, VWALL // heads), BF),
            dma((17,)),
            dma((6,)), dma((6,)),
            dma((max(n_sp - 1, 1),)), dma((max(n_sp - 1, 1),)),
            dma((3,)), dma((3,)),
            dma((chunk_sems,)), dma((chunk_sems,)),
            dma((6,)), dma((6,)),
            dma((3,)), dma((3,)),
            dma((8,)), dma((8,)),
            dma(()), dma(()),
        ],
        compiler_params=pltpu.CompilerParams(
            collective_id=0, has_side_effects=True, vmem_limit_bytes=66_100_000
        ),
        name="block",
    )(
        latent, context, cond, context_cond, norm_gain, mod_shift, mod_scale,
        mod_gate, w_query, w_key, w_value, query_gain, key_gain, value_gain, mix_lambda, context_lift, w_out,
        jnp.asarray(cos), jnp.asarray(sin),
    )
    return (latent.astype(F32) + update).astype(latent.dtype)


def solution(mesh):
    placed = (
        P(("dp", "sp", "tp"), None),
        P(("dp", "sp"), None),
        P(("dp", "sp")),
        P("sp"),
        P(),
        P("sp", "tp"),
        P("sp", "tp"),
        P("sp", "tp"),
        P(None, "tp"),
        P(None, "tp"),
        P(None, "tp"),
        P(),
        P(),
        P("tp"),
        P("tp"),
        P(),
        P("tp", None),
    )
    sizes = mesh.shape
    return jax.shard_map(
        functools.partial(on_device, sizes["sp"], sizes["tp"], sizes["dp"]),
        mesh=mesh,
        in_specs=placed,
        out_specs=P(("dp", "sp", "tp"), None),
        check_vma=False,
    )
```

profile of v0, /device:TPU:0, one launch (start us, length us, event | category | flops | bytes accessed | tf_op | source)
XLA Modules:
  0.0 40.6 jit_solution(9223402223523752744)
XLA Ops:
  0.0 0.0 copy-start
  0.0 39.8 %block.1 = f32[64,2048]{1,0:T(8,128)S(1)} custom-call(bf16[64,2048]{1,0:T(8,128)(2,1)} %refs_0_.1, bf16[64,2048]{1,0:T(8,128)(2,1)} %refs_1_.1, bf16[512]{0:T(512)(128)(2,1)} %refs_2_.1, bf16[512]{0:T(512)(128)(2,1)} %refs_3_.1, f32[2048]{0:T(1024)} %refs_4_.1, bf16[512,512]{1,0:T(8,128)(2,1)} %refs_5_.1, bf16[512,512]{1,0:T(8,128)(2,1)} %refs_6_.1, ...), custom_call_target="tpu_custom_call" | custom-call | tf_op jit(solution)/shard_map/block/pallas_call | solution.py:499
  39.8 0.0 copy-done
  39.8 0.8 %add_convert_fusion = bf16[64,2048]{1,0:T(8,128)(2,1)} fusion(f32[64,2048]{1,0:T(8,128)S(1)} %block.1, bf16[64,2048]{1,0:T(8,128)(2,1)S(1)} %copy-done), kind=kLoop, calls=%fused_computation | loop fusion | flops 393216 | bytes 1048576 | tf_op jit(solution)/shard_map/convert_element_type | solution.py:556
Async XLA Ops:
  0.0 39.8 %copy-start = (bf16[64,2048]{1,0:T(8,128)(2,1)S(1)}, bf16[64,2048]{1,0:T(8,128)(2,1)}, u32[]{:S(2)}) copy-start(bf16[64,2048]{1,0:T(8,128)(2,1)} %refs_0_.1) | copy-start | bytes 786436
where the time goes:
time: 40.7 us; the launch traced here: 40.6 us
  Pallas kernels  39.8 us (98%)
  other arithmetic  0.75 us (2%)
    pallas_call x1, Pallas kernels, on_device(): pl.pallas_call(functools.partial(kernel, n_sp, n_tp, n_dp, head_width), o...  39.8 us

commit v1 on v0

--- a/solution.py
+++ b/solution.py
@@ -36,7 +36,7 @@
         out_r,
         cond_r, cctx_r, gain_r, qg_r, kg_r, vg_r,
         lat, ctx, mw, wq, wk, wv, wo, cosv, sinv,
-        act, part, mod_in, summed, mod_full, vecs, invs, normed, qown, qin, qm, kvl, kvr, acc, mine, ho,
+        act, part, mod_in, summed, mod_full, vecs, invs, normed, qown, qin, qm, kvl, kvr, acc, mine, ho, grp,
         loc, bs_lat, br_lat, bs_mod, br_mod, bs_mt, br_mt, bs_kv, br_kv, bs_wo, br_wo,
         bs_dd, br_dd, bs_ho, br_ho, bs_q, br_q,
     ) = refs
@@ -67,22 +67,9 @@
         c.start()
         return c
 
-    l_one = [
-        local(11 + j, src, dst)
-        for j, (src, dst) in enumerate(
-            ((cond_h, cond_r), (cctx_h, cctx_r), (gain_h, gain_r), (qg_h, qg_r), (kg_h, kg_r),
-             (vg_h, vg_r))
-        )
-    ]
     l_lat = local(0, lat_h, lat.at[0])
+    l_one = [local(11 + j, src, dst) for j, (src, dst) in enumerate(((cond_h, cond_r), (cctx_h, cctx_r)))]
     l_mod = [local(1 + j, h, mw.at[j]) for j, h in enumerate((ms_h, msc_h, mg_h))]
-    l_ctx = local(4, ctx_h, ctx)
-    l_wk = local(5, wk_h, wk)
-    l_wv = local(6, wv_h, wv)
-    l_wq = local(7, wq_h, wq)
-    l_wo = local(8, wo_h, wo.at[0])
-    l_cos = local(9, cos_h.at[pl.ds(s * ROWS, ROWS)], cosv)
-    l_sin = local(10, sin_h.at[pl.ds(s * ROWS, ROWS)], sinv)
 
     bar = pltpu.get_barrier_semaphore()
     for k in range(1, n_sp):
@@ -93,6 +80,30 @@
             bar, inc=1, device_id={"sp": pair, "tp": peers[k]}, device_id_type=MESH
         )
     pl.semaphore_signal(bar, inc=1, device_id={"dp": partner}, device_id_type=MESH)
+
+    def remote(src, dst, ss, rs, where):
+        return pltpu.make_async_remote_copy(
+            src_ref=src, dst_ref=dst, send_sem=ss, recv_sem=rs, device_id=where, device_id_type=MESH
+        )
+
+    QR = HR // 2
+
+    def lat_copy(i, src_slot, dst_slot, at, count, where):
+        rows = pl.ds(at, count)
+        return remote(lat.at[src_slot, rows], lat.at[dst_slot, rows], bs_lat.at[i], br_lat.at[i],
+                      {"tp": where})
+
+    x0 = lat_copy(0, 0, 1, 0, HR, nbr1)
+    y1 = lat_copy(1, 0, 2, HR, HR, nbr2)
+    x1 = [lat_copy(2 + j, 0, 1, HR + j * QR, QR, nbr1) for j in range(2)]
+    y0 = [lat_copy(4 + j, 0, 2, j * QR, QR, nbr2) for j in range(2)]
+    f0 = lat_copy(6, 1, 3, 0, HR, nbr2)
+    f1 = lat_copy(7, 2, 3, HR, HR, nbr1)
+
+    l_lat.wait()
+    pl.semaphore_wait(bar, n_sp + 6)
+    for c in (x0, y1, x1[0], y0[0]):
+        c.start()
 
     act[...] = jnp.zeros_like(act)
     for row, ref in ((0, cond_r), (1, cctx_r)):
@@ -106,13 +117,6 @@
         res = jnp.dot(acts, mw[j], preferred_element_type=F32)
         part[2 * j : 2 * j + 2, :] = res[0:2]
 
-    pl.semaphore_wait(bar, n_sp + 6)
-
-    def remote(src, dst, ss, rs, where):
-        return pltpu.make_async_remote_copy(
-            src_ref=src, dst_ref=dst, send_sem=ss, recv_sem=rs, device_id=where, device_id_type=MESH
-        )
-
     mod_copies = []
     for k in range(1, n_sp):
         c = remote(part, mod_in.at[k - 1], bs_mod.at[k - 1], br_mod.at[k - 1],
@@ -120,21 +124,23 @@
         c.start()
         mod_copies.append(c)
 
-    l_lat.wait()
-
-    def lat_copy(i, src_slot, dst_slot, half, where):
-        rows = pl.ds(half * HR, HR)
-        return remote(lat.at[src_slot, rows], lat.at[dst_slot, rows], bs_lat.at[i], br_lat.at[i],
-                      {"tp": where})
-
-    x0 = lat_copy(0, 0, 1, 0, nbr1)
-    y1 = lat_copy(1, 0, 2, 1, nbr2)
-    x1 = lat_copy(2, 0, 1, 1, nbr1)
-    y0 = lat_copy(3, 0, 2, 0, nbr2)
-    f0 = lat_copy(4, 1, 3, 0, nbr2)
-    f1 = lat_copy(5, 2, 3, 1, nbr1)
-    for c in (x0, y1):
-        c.start()
+    l_ctx = local(4, ctx_h, ctx)
+    l_wk = local(5, wk_h, wk)
+    l_wv = local(6, wv_h, wv)
+    l_cos = local(9, cos_h.at[pl.ds(s * ROWS, ROWS)], cosv)
+    l_sin = local(10, sin_h.at[pl.ds(s * ROWS, ROWS)], sinv)
+    l_one += [
+        local(13 + j, src, dst)
+        for j, (src, dst) in enumerate(((gain_h, gain_r), (qg_h, qg_r), (kg_h, kg_r), (vg_h, vg_r)))
+    ]
+    l_wq = local(7, wq_h, wq)
+    l_wo = local(8, wo_h, wo.at[0])
+
+    group = (
+        lax.rem(lax.broadcasted_iota(jnp.int32, (2 * QW, QW), 0), QW) // head_width
+        == lax.broadcasted_iota(jnp.int32, (2 * QW, QW), 1) // head_width
+    )
+    grp[...] = jnp.where(group, 1.0 / head_width, 0.0).astype(BF)
 
     l_ctx.wait()
 
@@ -158,12 +164,50 @@
         c = remote(summed, mod_full.at[t], bs_mt.at[k - 1], br_mt.at[k - 1], {"tp": peers[k]})
         c.start()
         tp_copies.append(c)
-    x1.start()
-    y0.start()
+    x1[1].start()
+    y0[1].start()
     x0.wait_recv()
     f0.start()
     y1.wait_recv()
     f1.start()
+
+    HALF = wo.shape[1] // 2
+    QUART = HALF // 2
+    EIGHTH = QUART // 2
+
+    def wo_rows(at, count):
+        return pl.ds(pl.multiple_of(core * HALF + at, count), count)
+
+    def wo_copy(i, src_slot, dst_slot, at, count, where):
+        rows = wo_rows(at, count)
+        return remote(wo.at[src_slot, rows], wo.at[dst_slot, rows], bs_wo.at[i], br_wo.at[i],
+                      {"tp": where})
+
+    def dd_copy(i, k, at, count):
+        rows = wo_rows(at, count)
+        return remote(wo.at[k, rows], wo.at[k, rows], bs_dd.at[i], br_dd.at[i], {"dp": partner})
+
+    def dd_recv(i, k, at, count):
+        rows = pl.ds(pl.multiple_of((1 - core) * HALF + at, count), count)
+        return remote(wo.at[k, rows], wo.at[k, rows], bs_dd.at[i], br_dd.at[i], {"dp": partner})
+
+    wx0 = wo_copy(0, 0, 1, 0, QUART, nbr1)
+    wy1 = wo_copy(1, 0, 2, QUART, QUART, nbr2)
+    wx1 = wo_copy(2, 0, 1, QUART, QUART, nbr1)
+    wy0 = wo_copy(3, 0, 2, 0, QUART, nbr2)
+    wf = [
+        wo_copy(4, 1, 3, 0, EIGHTH, nbr2),
+        wo_copy(5, 1, 3, EIGHTH, EIGHTH, nbr2),
+        wo_copy(6, 2, 3, QUART, EIGHTH, nbr1),
+        wo_copy(7, 2, 3, QUART + EIGHTH, EIGHTH, nbr1),
+    ]
+    dd_parts = [(0, 1, 0, HALF), (1, 2, 0, HALF), (2, 3, 0, EIGHTH), (3, 3, EIGHTH, EIGHTH),
+                (4, 3, QUART, EIGHTH), (5, 3, QUART + EIGHTH, EIGHTH)]
+    dd = [dd_copy(*d) for d in dd_parts]
+
+    l_wo.wait()
+    for c in (wx0, wy1, wx1, wy0):
+        c.start()
 
     for k in range(1, 4):
         remote(summed, mod_full.at[peers[k]], bs_mt.at[k - 1], br_mt.at[k - 1],
@@ -186,33 +230,6 @@
     vecs[3:4, :] = gain * (1.0 + full_row(3))
     vecs[4:5, :] = full_row(4)
 
-    HALF = wo.shape[1] // 2
-    QUART = HALF // 2
-
-    def wo_rows(q):
-        return pl.ds(pl.multiple_of(core * HALF + q * QUART, QUART), QUART)
-
-    def wo_copy(i, src_slot, dst_slot, q, where):
-        return remote(wo.at[src_slot, wo_rows(q)], wo.at[dst_slot, wo_rows(q)], bs_wo.at[i],
-                      br_wo.at[i], {"tp": where})
-
-    def dd_copy(k):
-        rows = pl.ds(pl.multiple_of(core * HALF, HALF), HALF)
-        return remote(wo.at[k, rows], wo.at[k, rows], bs_dd.at[k - 1], br_dd.at[k - 1],
-                      {"dp": partner})
-
-    def dd_recv(k):
-        rows = pl.ds(pl.multiple_of((1 - core) * HALF, HALF), HALF)
-        return remote(wo.at[k, rows], wo.at[k, rows], bs_dd.at[k - 1], br_dd.at[k - 1],
-                      {"dp": partner})
-
-    wx0 = wo_copy(0, 0, 1, 0, nbr1)
-    wy1 = wo_copy(1, 0, 2, 1, nbr2)
-    wx1 = wo_copy(2, 0, 1, 1, nbr1)
-    wy0 = wo_copy(3, 0, 2, 0, nbr2)
-    wf0 = wo_copy(4, 1, 3, 0, nbr2)
-    wf1 = wo_copy(5, 2, 3, 1, nbr1)
-
     def norm_rows(src, row, count, dst_at):
         step = 16
 
@@ -233,14 +250,11 @@
                 v * invs[at, 0:1] * vecs[2 + row : 3 + row, :] + vecs[row : row + 1, :]
             ).astype(BF)
 
-    group = (
-        lax.broadcasted_iota(jnp.int32, (QW, QW), 0) // head_width
-        == lax.broadcasted_iota(jnp.int32, (QW, QW), 1) // head_width
-    )
-    group = jnp.where(group, 1.0 / head_width, 0.0).astype(F32)
-
     def head_norm(x):
-        mean = jnp.dot(x * x, group, precision=lax.Precision.HIGHEST, preferred_element_type=F32)
+        square = x * x
+        high = square.astype(BF)
+        low = (square - high.astype(F32)).astype(BF)
+        mean = jnp.dot(jnp.concatenate([high, low], axis=1), grp[...], preferred_element_type=F32)
         return x * lax.rsqrt(mean + token_eps)
 
     def turn(y, cos, sin):
@@ -253,18 +267,22 @@
         )
         return y * cos + other * sin
 
-    def project_block(k, first):
-        rows = pl.ds(first + C, R)
-        x = normed[C + k * R : C + (k + 1) * R, :]
-        at = pl.ds(pl.multiple_of(peers[k] * R, R), R)
-        cos, sin = cosv[at, :], sinv[at, :]
+    def project(first, count, plain):
+        x = normed[first : first + count, :]
         kk = head_norm(jnp.dot(x, wk[...], preferred_element_type=F32))
         for h in range(n_head):
             y = kk[:, h * HW : (h + 1) * HW] * k_gain
-            kvl[h, rows, 0:HW] = turn(y, cos, sin).astype(BF)
+            if plain:
+                kvl[h, first : first + plain, 0:HW] = y[:plain].astype(BF)
+            for at in range(plain, count, R):
+                k = (first + at - C) // R
+                pos = pl.ds(pl.multiple_of(peers[k] * R, R), R)
+                kvl[h, first + at : first + at + R, 0:HW] = turn(
+                    y[at : at + R], cosv[pos, :], sinv[pos, :]
+                ).astype(BF)
         vv = jnp.dot(x, wv[...], preferred_element_type=F32).astype(BF)
         for h in range(n_head):
-            kvl[h, rows, HW:] = vv[:, h * VW : (h + 1) * VW]
+            kvl[h, first : first + count, HW:] = vv[:, h * VW : (h + 1) * VW]
 
     def project_queries():
         x = normed[C:, :]
@@ -329,29 +347,19 @@
     l_wv.wait()
     l_cos.wait()
     l_sin.wait()
-    x = normed[0:C, :]
-    kk = head_norm(jnp.dot(x, wk[...], preferred_element_type=F32))
-    vv = jnp.dot(x, wv[...], preferred_element_type=F32).astype(BF)
-    for h in range(n_head):
-        kvl[h, 0:C, 0:HW] = (kk[:, h * HW : (h + 1) * HW] * k_gain).astype(BF)
-        kvl[h, 0:C, HW:] = vv[:, h * VW : (h + 1) * VW]
-    project_block(0, 0)
+    project(0, C + R, C)
     send_own(0)
 
-    x1.wait_recv()
-    y0.wait_recv()
-    l_wo.wait()
-    for c in (wx0, wy1, wx1, wy0):
-        c.start()
+    for c in [x1[0], x1[1], y0[0], y0[1]]:
+        c.wait_recv()
     norm_rows(lat.at[1], 0, R, C + R)
     norm_rows(lat.at[2], 0, R, C + 2 * R)
-    project_block(1, R)
-    project_block(2, 2 * R)
+    project(C + R, 2 * R, 0)
     send_own(1)
     f0.wait_recv()
     f1.wait_recv()
     norm_rows(lat.at[3], 0, R, C + 3 * R)
-    project_block(3, 3 * R)
+    project(C + 3 * R, R, 0)
     send_own(2)
 
     def arrive(dist, c):
@@ -409,9 +417,11 @@
     for c in range(1, len(chunks)):
         arrive(1, c)
     wx0.wait_recv()
-    wf0.start()
+    wf[0].start()
+    wf[1].start()
     wy1.wait_recv()
-    wf1.start()
+    wf[2].start()
+    wf[3].start()
     q_copy.wait_recv()
     split_maps(qin[...], ROWS)
     attend(kvl.at[e], 0, C + ROWS, ROWS, ROWS, True)
@@ -421,22 +431,20 @@
         if dist > 1:
             for c in range(len(chunks)):
                 arrive(dist, c)
-                if last:
-                    attend_arrived(dist, *chunks[c])
-        if not last:
-            attend_arrived(dist, 0, C + ROWS)
+        attend_arrived(dist, 0, C + ROWS)
         if dist == 2 or (last and n_sp == 2):
             wx1.wait_recv()
-            dd_copy(1).start()
+            dd[0].start()
             wy0.wait_recv()
-            dd_copy(2).start()
+            dd[1].start()
 
     def ho_copy(q, k):
         i = q * 4 + k
         where = {"tp": peers[k]} if q == 0 else {"sp": pair, "tp": peers[k]}
         if q == 1 and k == 0:
             where = {"sp": pair}
-        return remote(mine.at[q, k], ho.at[q, k], bs_ho.at[i], br_ho.at[i], where)
+        lanes = pl.ds(pl.multiple_of(e * VW, VW), VW)
+        return remote(mine.at[q, k], ho.at[k, :, lanes], bs_ho.at[i], br_ho.at[i], where)
 
     for q, k in ((1, 3), (1, 1), (1, 2), (0, 3), (1, 0), (0, 1), (0, 2), (0, 0)):
         rows = slice((4 * q + k) * R, (4 * q + k + 1) * R)
@@ -444,29 +452,37 @@
         a1 = acc[1, rows, :]
         mixed = a0[:, :VW] / a0[:, VW:] - lam_r[e] * (a1[:, :VW] / a1[:, VW:])
         inv = lax.rsqrt(jnp.mean(mixed * mixed, axis=-1, keepdims=True) + head_eps)
-        mine[q, k, :, :] = (mixed * inv * v_gain * head_factor).astype(BF)
+        value = (mixed * inv * v_gain * head_factor).astype(BF)
         if q or k:
+            mine[q, k, :, :] = value
             ho_copy(q, k).start()
-
-    wf0.wait_recv()
-    wf1.wait_recv()
-    dd_copy(3).start()
-
-    def head_rows(q):
-        return pl.ds(pl.multiple_of((e if q == 0 else 1 - e) * VW, VW), VW)
-
-    out = jnp.dot(mine[0, 0], wo[0, head_rows(0), :], preferred_element_type=F32)
-    for q, k in ((0, 1), (0, 2), (1, 0), (0, 3), (1, 1), (1, 2), (1, 3)):
-        if q == 0:
-            dd_recv(k).wait_recv()
-        ho_copy(q, k).wait_recv()
-        out += jnp.dot(ho[q, k], wo[k, head_rows(q), :], preferred_element_type=F32)
-    out_r[...] = vecs[4:5, :] * out
-
-    for c in mod_copies + tp_copies + [x0, y1, x1, y0, f0, f1, wx0, wy1, wx1, wy0, wf0, wf1]:
+        else:
+            for h in range(2):
+                @pl.when(e == h)
+                def _():
+                    ho[0, :, h * VW : (h + 1) * VW] = value
+
+    for c, d in zip(wf, dd[2:]):
+        c.wait_recv()
+        d.start()
+
+    for k in range(4):
+        for i, part_k, at, count in dd_parts:
+            if part_k == k:
+                dd_recv(i, k, at, count).wait_recv()
+        for q in range(2):
+            if q or k:
+                ho_copy(q, k).wait_recv()
+        add = jnp.dot(ho[k], wo[k], preferred_element_type=F32)
+        if k == 0:
+            out_r[...] = add
+        elif k < 3:
+            out_r[...] += add
+        else:
+            out_r[...] = vecs[4:5, :] * (out_r[...] + add)
+
+    for c in mod_copies + tp_copies + [x0, y1, *x1, *y0, f0, f1, wx0, wy1, wx1, wy0] + wf + dd:
         c.wait_send()
-    for k in range(1, 4):
-        dd_copy(k).wait_send()
     q_copy.wait_send()
     for q in range(2):
         for k in range(4):
@@ -533,14 +549,15 @@
             pltpu.VMEM((n_sp, C + ROWS, (QW + VWALL) // heads), BF),
             pltpu.VMEM((2, 2 * ROWS, 2 * VWALL // heads), F32),
             pltpu.VMEM((2, 4, R, VWALL // heads), BF),
-            pltpu.VMEM((2, 4, R, VWALL // heads), BF),
+            pltpu.VMEM((4, R, VWALL), BF),
+            pltpu.VMEM((2 * QW, QW), BF),
             dma((17,)),
-            dma((6,)), dma((6,)),
+            dma((8,)), dma((8,)),
             dma((max(n_sp - 1, 1),)), dma((max(n_sp - 1, 1),)),
             dma((3,)), dma((3,)),
             dma((chunk_sems,)), dma((chunk_sems,)),
+            dma((8,)), dma((8,)),
             dma((6,)), dma((6,)),
-            dma((3,)), dma((3,)),
             dma((8,)), dma((8,)),
             dma(()), dma(()),
         ],

time: 40.7 us -> 38.5 us (0.946)
  Pallas kernels: 39.8 us -> 37.5 us
    pallas_call x1, Pallas kernels: 39.8 us -> 37.5 us  [on_device(): pl.pallas_call(functools.partial(kernel, n_sp, n_tp, n_dp, head_width), o...]
where the time goes in v1:
time: 38.5 us; the launch traced here: 38.3 us
  Pallas kernels  37.5 us (97%)
  other arithmetic  0.75 us (2%)
    pallas_call x1, Pallas kernels, on_device(): pl.pallas_call(functools.partial(kernel, n_sp, n_tp, n_dp, head_width), o...  37.5 us

profile of v1, /device:TPU:0, one launch (start us, length us, event | category | flops | bytes accessed | tf_op | source)
XLA Modules:
  0.0 38.3 jit_solution(14028999583874898227)
XLA Ops:
  0.0 0.0 copy-start
  0.0 37.5 %block.1 = f32[64,2048]{1,0:T(8,128)S(1)} custom-call(bf16[64,2048]{1,0:T(8,128)(2,1)} %refs_0_.1, bf16[64,2048]{1,0:T(8,128)(2,1)} %refs_1_.1, bf16[512]{0:T(512)(128)(2,1)} %refs_2_.1, bf16[512]{0:T(512)(128)(2,1)} %refs_3_.1, f32[2048]{0:T(1024)} %refs_4_.1, bf16[512,512]{1,0:T(8,128)(2,1)} %refs_5_.1, bf16[512,512]{1,0:T(8,128)(2,1)} %refs_6_.1, ...), custom_call_target="tpu_custom_call" | custom-call | tf_op jit(solution)/shard_map/block/pallas_call | solution.py:515
  37.5 0.0 copy-done
  37.5 0.8 %add_convert_fusion = bf16[64,2048]{1,0:T(8,128)(2,1)} fusion(f32[64,2048]{1,0:T(8,128)S(1)} %block.1, bf16[64,2048]{1,0:T(8,128)(2,1)S(1)} %copy-done), kind=kLoop, calls=%fused_computation | loop fusion | flops 393216 | bytes 1048576 | tf_op jit(solution)/shard_map/convert_element_type | solution.py:573
Async XLA Ops:
  0.0 37.5 %copy-start = (bf16[64,2048]{1,0:T(8,128)(2,1)S(1)}, bf16[64,2048]{1,0:T(8,128)(2,1)}, u32[]{:S(2)}) copy-start(bf16[64,2048]{1,0:T(8,128)(2,1)} %refs_0_.1) | copy-start | bytes 786436

commit v2 on v1

v2 whole, which is shorter than its diff:
```python
import functools

import jax
import jax.numpy as jnp
import numpy as np
from jax import lax
from jax.experimental import pallas as pl
from jax.experimental.pallas import tpu as pltpu
from jax.sharding import PartitionSpec as P

GRID = 64
token_eps = 0.01
head_eps = 0.001
rope_base = 10000.0
head_factor = 0.8
MESH = pl.DeviceIdType.MESH
BF = jnp.bfloat16
F32 = jnp.float32


def rope_tables(length, width):
    quarter = width // 4
    inverse = (rope_base ** (-np.arange(quarter, dtype=np.float64) / quarter)).astype(np.float32)
    pos = np.arange(length)
    row = (pos // GRID).astype(np.float32)[:, None] * inverse
    col = (pos % GRID).astype(np.float32)[:, None] * inverse
    cos = np.concatenate([np.cos(row), np.cos(row), np.cos(col), np.cos(col)], axis=1)
    sin = np.concatenate([-np.sin(row), np.sin(row), -np.sin(col), np.sin(col)], axis=1)
    return np.tile(cos, (1, 2)).astype(np.float32), np.tile(sin, (1, 2)).astype(np.float32)


def kernel(n_sp, n_tp, n_dp, head_width, *refs):
    (
        lat_h, ctx_h, cond_h, cctx_h, gain_h, ms_h, msc_h, mg_h, wq_h, wk_h, wv_h,
        qg_h, kg_h, vg_h, lam_r, lift_r, wo_h, cos_h, sin_h,
        out_r,
        cond_r, cctx_r, gain_r, qg_r, kg_r, vg_r,
        own, lat, ctx, mw, wq, wkv, wo, turns,
        act, part, mod_in, summed, mod_full, vecs, normed, qown, qin, qm, kvl, kvr, kvc, acc,
        mine, ho, grp,
        loc, s_swap, r_swap, s_lat, r_lat, s_mod, r_mod, s_mt, r_mt, s_vec, r_vec, s_kv, r_kv,
        s_ctx, r_ctx, s_q, r_q, s_wo, r_wo, s_dd, r_dd, s_ho, r_ho,
    ) = refs
    s = lax.axis_index("sp")
    t = lax.axis_index("tp")
    d_ix = lax.axis_index("dp")
    core = lax.rem(d_ix, 2)
    partner = d_ix + 1 - 2 * core
    t_odd = lax.rem(t, 2)
    nbr1 = t + 1 - 2 * t_odd
    nbr2 = lax.rem(t + 2, 4)
    nbr3 = lax.rem(nbr1 + 2, 4)
    peers = (t, nbr1, nbr2, nbr3)
    H = n_sp // 2
    half = s // H
    base = half * H
    s_opp = lax.rem(s + H, n_sp)
    home = core == half
    away = jnp.not_equal(core, half)
    a = lax.rem(core + half, 2)
    block = s + a * (s_opp - s)
    other_block = s_opp + a * (s - s_opp)
    d_work = d_ix - core + half
    R, D = own.shape
    PR = R // 4
    C = ctx.shape[0]
    QW = wq.shape[1]
    n_head = QW // (2 * head_width)
    HW = 2 * head_width
    VW = wkv.shape[2] // n_head
    ROWS = 4 * R

    bar = pltpu.get_barrier_semaphore()
    greeted = [{"tp": peers[k]} for k in range(1, 4)] + [{"dp": partner}]
    for k in range(1, n_sp):
        there = lax.rem(s + k, n_sp)
        greeted += [{"sp": there}, {"dp": partner, "sp": there}]
    for where in greeted:
        pl.semaphore_signal(bar, inc=1, device_id=where, device_id_type=MESH)

    def local(i, src, dst):
        c = pltpu.make_async_copy(src, dst, loc.at[i])
        c.start()
        return c

    def remote(src, dst, ss, rs, where):
        return pltpu.make_async_remote_copy(
            src_ref=src, dst_ref=dst, send_sem=ss, recv_sem=rs, device_id=where, device_id_type=MESH
        )

    def drain(ref, sem):
        remote(ref, ref, sem, sem, {"dp": partner}).wait_recv()

    @pl.when(home)
    def _():
        local(0, lat_h, lat.at[0])

    @pl.when(away)
    def _():
        local(0, lat_h, own)

    l_one = [local(1, cond_h, cond_r), local(2, cctx_h, cctx_r)]
    for j, h in enumerate((ms_h, msc_h, mg_h)):
        local(3, h, mw.at[j])

    act[...] = jnp.zeros_like(act)
    for row, ref in ((0, cond_r), (1, cctx_r)):
        l_one[row].wait()
        v = ref[...].astype(F32).reshape(1, -1)
        act[row : row + 1, :] = v / (1.0 + jnp.exp(-v))
    acts = act[...].astype(BF)
    part[...] = jnp.zeros_like(part)
    drain(mw, loc.at[3])
    for j in range(3):
        res = jnp.dot(acts, mw[j], preferred_element_type=F32)
        part[2 * j : 2 * j + 2, :] = res[0:2]

    drain(own, loc.at[0])
    pl.semaphore_wait(bar, len(greeted))

    def mod_copy(k):
        return remote(part, mod_in.at[k - 1], s_mod, r_mod, {"sp": lax.rem(s + k, n_sp)})

    def piece(j):
        return pl.ds(j * PR, PR)

    def swap(j):
        return remote(own.at[piece(j)], lat.at[0, piece(j)], s_swap, r_swap.at[j],
                      {"dp": partner, "sp": s_opp})

    def along_x(j):
        return remote(lat.at[0, piece(j)], lat.at[1, piece(j)], s_lat, r_lat.at[j if j < 2 else 4],
                      {"tp": nbr1})

    def along_y(j):
        return remote(lat.at[0, piece(j)], lat.at[2, piece(j)], s_lat, r_lat.at[j if j > 1 else 4],
                      {"tp": nbr2})

    def onward(j):
        slot, where = (1, nbr2) if j < 2 else (2, nbr1)
        return remote(lat.at[slot, piece(j)], lat.at[3, piece(j)], s_lat, r_lat.at[5], {"tp": where})

    def pass_on(j):
        (along_x(j) if j < 2 else along_y(j)).wait_recv()
        onward(j).start()

    for k in range(1, n_sp):
        mod_copy(k).start()

    @pl.when(home)
    def _():
        for j in range(4):
            along_x(j).start()
            along_y((j + 2) % 4).start()

    @pl.when(away)
    def _():
        swap(0).start()
        swap(1).start()

    l_ctx = local(4, ctx_h, ctx)
    local(5, wk_h, wkv.at[0])
    local(5, wv_h, wkv.at[1])
    at_turns = pl.ds(pl.multiple_of(block * ROWS, ROWS), ROWS)
    local(6, cos_h.at[at_turns], turns.at[0])
    local(6, sin_h.at[at_turns], turns.at[1])
    l_small = [
        local(7 + j, src, dst)
        for j, (src, dst) in enumerate(((gain_h, gain_r), (qg_h, qg_r), (kg_h, kg_r), (vg_h, vg_r)))
    ]
    l_wq = local(11, wq_h, wq)
    l_wo = local(12, wo_h, wo.at[0])

    group = (
        lax.rem(lax.broadcasted_iota(jnp.int32, (2 * QW, QW), 0), QW) // head_width
        == lax.broadcasted_iota(jnp.int32, (2 * QW, QW), 1) // head_width
    )
    grp[...] = jnp.where(group, 1.0 / head_width, 0.0).astype(BF)
    for c in l_small:
        c.wait()
    gain = gain_r[...].reshape(1, -1)
    q_gain = qg_r[...].reshape(1, -1)
    q_gain = jnp.concatenate([q_gain, q_gain], axis=1)
    k_gain = kg_r[...].reshape(1, -1)
    k_gain = jnp.concatenate([k_gain, k_gain], axis=1)
    v_gain = vg_r[...].reshape(1, -1)

    drain(mod_in, r_mod)
    total = part[...]
    for k in range(n_sp - 1):
        total = total + mod_in[k]
    summed[...] = total
    mod_full[t] = total

    def mt_copy(k):
        return remote(summed, mod_full.at[t], s_mt, r_mt, {"tp": peers[k]})

    for k in range(1, 4):
        mt_copy(k).start()

    HALF = wo.shape[1] // 2
    QUART = HALF // 2
    EIGHTH = QUART // 2

    def wo_rows(at, count):
        return pl.ds(pl.multiple_of(core * HALF + at, count), count)

    def wo_copy(i, src_slot, dst_slot, at, count, where):
        rows = wo_rows(at, count)
        return remote(wo.at[src_slot, rows], wo.at[dst_slot, rows], s_wo, r_wo.at[i], {"tp": where})

    def dd_copy(i, k, at, count):
        rows = wo_rows(at, count)
        return remote(wo.at[k, rows], wo.at[k, rows], s_dd, r_dd.at[i], {"dp": partner})

    wx0 = wo_copy(0, 0, 1, 0, QUART, nbr1)
    wy1 = wo_copy(1, 0, 2, QUART, QUART, nbr2)
    wx1 = wo_copy(2, 0, 1, QUART, QUART, nbr1)
    wy0 = wo_copy(2, 0, 2, 0, QUART, nbr2)
    wf = [
        wo_copy(3, 1, 3, 0, EIGHTH, nbr2),
        wo_copy(4, 1, 3, EIGHTH, EIGHTH, nbr2),
        wo_copy(5, 2, 3, QUART, EIGHTH, nbr1),
        wo_copy(6, 2, 3, QUART + EIGHTH, EIGHTH, nbr1),
    ]
    dd = [dd_copy(0, 1, 0, HALF), dd_copy(1, 2, 0, HALF)] + [
        dd_copy(2, 3, i * EIGHTH, EIGHTH) for i in range(4)
    ]
    l_wo.wait()

    @pl.when(home)
    def _():
        for j in (0, 2, 1, 3):
            pass_on(j)
        for c in (wx0, wy1, wx1, wy0):
            c.start()

    @pl.when(away)
    def _():
        swap(2).start()
        swap(3).start()
        for j in range(4):
            swap(j).wait_recv()
            along_x(j).start()
            along_y(j).start()
        pass_on(0)
        pass_on(1)

    drain(mod_full.at[0:3], r_mt)

    def full_row(j):
        return jnp.concatenate([mod_full[q, j : j + 1, :] for q in range(n_tp)], axis=1)

    vecs[0, 0:1, :] = full_row(0)
    vecs[0, 1:2, :] = full_row(1)
    vecs[0, 2:3, :] = gain * (1.0 + full_row(2))
    vecs[0, 3:4, :] = gain * (1.0 + full_row(3))
    vecs[0, 4:8, :] = jnp.broadcast_to(full_row(4), (4, D))
    vec_copy = remote(vecs.at[0], vecs.at[1], s_vec, r_vec, {"dp": partner})

    @pl.when(home)
    def _():
        vec_copy.start()

    @pl.when(away)
    def _():
        vec_copy.wait_recv()

    def norm_rows(src, row, count, dst_at):
        step = 16

        @pl.loop(0, count // step, unroll=True)
        def _(i):
            at = pl.multiple_of(i * step, step)
            v = src[pl.ds(at, step), :].astype(F32)
            inv = lax.rsqrt(jnp.mean(v * v, axis=-1, keepdims=True) + token_eps)
            normed[pl.ds(dst_at + at, step), :] = (
                v * inv * vecs[a, 2 + row : 3 + row, :] + vecs[a, row : row + 1, :]
            ).astype(BF)

    def head_norm(x):
        square = x * x
        high = square.astype(BF)
        low = (square - high.astype(F32)).astype(BF)
        mean = jnp.dot(jnp.concatenate([high, low], axis=1), grp[...], preferred_element_type=F32)
        return x * lax.rsqrt(mean + token_eps)

    def turn(y, cos, sin):
        lane = lax.broadcasted_iota(jnp.int32, y.shape, 1)
        front = lax.rem(lane, head_width // 2) < head_width // 4
        other = jnp.where(
            front,
            pltpu.roll(y, HW - head_width // 4, axis=1),
            pltpu.roll(y, head_width // 4, axis=1),
        )
        return y * cos + other * sin

    def turns_of(k):
        at = pl.ds(pl.multiple_of(peers[k] * R, R), R)
        return turns[0, at, :], turns[1, at, :]

    def project(first, count, plain):
        x = normed[first : first + count, :]
        kk = head_norm(jnp.dot(x, wkv[0], preferred_element_type=F32))
        for h in range(n_head):
            y = kk[:, h * HW : (h + 1) * HW] * k_gain
            if plain:
                kvl[h, first : first + plain, 0:HW] = y[:plain].astype(BF)
            for at in range(plain, count, R):
                kvl[h, first + at : first + at + R, 0:HW] = turn(
                    y[at : at + R], *turns_of((first + at - C) // R)
                ).astype(BF)
        vv = jnp.dot(x, wkv[1], preferred_element_type=F32).astype(BF)
        for h in range(n_head):
            kvl[h, first : first + count, HW:] = vv[:, h * VW : (h + 1) * VW]

    def project_queries():
        x = normed[C:, :]
        qq = head_norm(jnp.dot(x, wq[...], preferred_element_type=F32))
        for k in range(4):
            for h in range(n_head):
                y = qq[k * R : (k + 1) * R, h * HW : (h + 1) * HW] * q_gain
                qown[h, k * R : (k + 1) * R, :] = (
                    turn(y, *turns_of(k)) * (head_width ** -0.5)
                ).astype(BF)

    def split_maps(q, at):
        lane = lax.broadcasted_iota(jnp.int32, q.shape, 1)
        for m in range(2):
            qm[m, at : at + ROWS, :] = jnp.where(lane // head_width == m, q, jnp.zeros_like(q))

    def kv_copy(j, head, at, count):
        there = base + lax.rem(s - base + j, H)
        i = 2 * j + a
        return remote(kvl.at[head, pl.ds(C + at, count)], kvr.at[block, pl.ds(at, count)], s_kv,
                      r_kv.at[i], {"dp": d_ix - core + head, "sp": there})

    def send_block(at, count):
        for j in range(1, H):
            for head in range(2):
                kv_copy(j, head, at, count).start()
        kv_copy(0, 1 - core, at, count).start()

    def ctx_copy(there, head):
        at = pl.ds(pl.multiple_of(s * C, C), C)
        return remote(kvl.at[head, pl.ds(0, C)], kvc.at[at], s_ctx, r_ctx,
                      {"dp": d_ix - core + head, "sp": there})

    def send_ctx():
        @pl.when(home)
        def _():
            for j in range(1, H):
                for head in range(2):
                    ctx_copy(base + lax.rem(s - base + j, H), head).start()
            ctx_copy(s, 1 - core).start()
            kvc[pl.ds(pl.multiple_of(s * C, C), C), :] = kvl[core, 0:C, :]

        @pl.when(away)
        def _():
            for j in range(H):
                for head in range(2):
                    ctx_copy(lax.rem(s_opp + j, H) + H - base, head).start()

    l_ctx.wait()
    norm_rows(ctx, 1, C, 0)
    norm_rows(lat.at[0], 0, R, C)
    drain(wkv, loc.at[5])
    drain(turns, loc.at[6])
    project(0, C + R, C)
    send_block(0, R)
    send_ctx()

    @pl.when(away)
    def _():
        pass_on(2)
        pass_on(3)
        for c in (wx0, wy1, wx1, wy0):
            c.start()

    drain(lat.at[1], r_lat.at[4])
    norm_rows(lat.at[1], 0, R, C + R)
    norm_rows(lat.at[2], 0, R, C + 2 * R)
    project(C + R, 2 * R, 0)
    send_block(R, 2 * R)
    drain(lat.at[3], r_lat.at[5])
    norm_rows(lat.at[3], 0, R, C + 3 * R)
    project(C + 3 * R, R, 0)
    send_block(3 * R, R)

    l_wq.wait()
    project_queries()
    q_copy = remote(qown.at[1 - core], qin, s_q, r_q, {"dp": partner})
    q_copy.start()
    split_maps(qown[core], 0)

    QB = 2 * R
    lift = lift_r[core]

    def attend(block, at, keys, start_row, count, first, plus):
        k = block[at : at + keys, 0:HW]
        v = block[at : at + keys, HW:]
        vx = jnp.concatenate([v, jnp.ones_like(v)], axis=1)
        for m in range(2):
            for b in range(count // QB):
                rows = slice(start_row + b * QB, start_row + (b + 1) * QB)
                sc = lax.dot_general(
                    qm[m, rows, :], k, (((1,), (1,)), ((), ())), preferred_element_type=F32
                )
                if plus is not None:
                    sc = sc + plus
                p = jnp.exp(sc).astype(BF)
                add = jnp.dot(p, vx, preferred_element_type=F32)
                if first:
                    acc[m, rows, :] = add
                else:
                    acc[m, rows, :] += add

    attend(kvl.at[core], C, ROWS, 0, ROWS, True, None)
    wx0.wait_recv()
    wf[0].start()
    wf[1].start()
    wy1.wait_recv()
    wf[2].start()
    wf[3].start()
    q_copy.wait_recv()
    split_maps(qin[...], ROWS)
    attend(kvl.at[core], C, ROWS, ROWS, ROWS, True, None)

    def attend_block(slot, i):
        drain(kvr.at[slot], r_kv.at[i])
        attend(kvr.at[slot], 0, ROWS, 0, 2 * ROWS, False, None)

    for j in range(1, H):
        attend_block(base + lax.rem(s - base + H - j, H), 2 * j)

    @pl.when(home)
    def _():
        drain(kvc.at[pl.ds(0, (n_sp - 1) * C)], r_ctx)

    @pl.when(away)
    def _():
        drain(kvc, r_ctx)

    attend(kvc, 0, n_sp * C, 0, 2 * ROWS, False, lift)
    attend_block(other_block, 1 - a)
    drain(wo.at[1, pl.ds(0, HALF)], r_wo.at[2])
    dd[0].start()
    dd[1].start()
    for j in range(1, H):
        attend_block(lax.rem(base + lax.rem(s - base + H - j, H) + H, n_sp), 2 * j + 1)

    def ho_copy(q, k):
        lanes = pl.ds(pl.multiple_of(core * VW, VW), VW)
        return remote(mine.at[4 * q + k], ho.at[k, :, lanes], s_ho, r_ho.at[k],
                      {"dp": d_work, "sp": other_block if q else block, "tp": peers[k]})

    for q, k in ((1, 3), (0, 3), (1, 1), (0, 1), (1, 2), (0, 2), (1, 0), (0, 0)):
        rows = slice((4 * q + k) * R, (4 * q + k + 1) * R)
        a0 = acc[0, rows, :]
        a1 = acc[1, rows, :]
        mixed = a0[:, :VW] / a0[:, VW:] - lam_r[core] * (a1[:, :VW] / a1[:, VW:])
        inv = lax.rsqrt(jnp.mean(mixed * mixed, axis=-1, keepdims=True) + head_eps)
        value = (mixed * inv * v_gain * head_factor).astype(BF)
        mine[4 * q + k, :, :] = value
        if q or k:
            ho_copy(q, k).start()
        else:
            @pl.when(away)
            def _():
                ho_copy(0, 0).start()

            for h in range(2):
                @pl.when(jnp.logical_and(home, core == h))
                def _():
                    ho[0, :, h * VW : (h + 1) * VW] = value

    for i in range(4):
        wf[i].wait_recv()
        dd[2 + i].start()

    @pl.when(home)
    def _():
        drain(mine.at[0], r_ho.at[0])

    @pl.when(away)
    def _():
        drain(ho.at[0], r_ho.at[0])

    for k in range(4):
        if k:
            drain(wo.at[k, pl.ds(0, HALF)], r_dd.at[k - 1])
            drain(ho.at[k], r_ho.at[k])
        add = jnp.dot(ho[k], wo[k], preferred_element_type=F32)
        if k == 0:
            out_r[...] = add
        elif k < 3:
            out_r[...] += add
        else:
            out_r[...] = vecs[0, 4:5, :] * (out_r[...] + add)

    def sent(ref, sem):
        remote(ref, ref, sem, sem, {"dp": partner}).wait_send()

    sent(mod_in, s_mod)
    sent(mod_full.at[0:3], s_mt)
    sent(lat.at[0:3], s_lat)
    sent(kvr.at[0 : n_sp - 1], s_kv)
    sent(wo.at[0:3, pl.ds(0, HALF)], s_wo)
    sent(wo.at[0:3, pl.ds(0, HALF)], s_dd)
    q_copy.wait_send()

    @pl.when(home)
    def _():
        vec_copy.wait_send()
        sent(kvc.at[pl.ds(0, (n_sp - 1) * C)], s_ctx)
        sent(mine.at[1:8], s_ho)

    @pl.when(away)
    def _():
        sent(own, s_swap)
        sent(kvc, s_ctx)
        sent(mine, s_ho)


def on_device(n_sp, n_tp, n_dp, *args):
    (
        latent, context, cond, context_cond, norm_gain, mod_shift, mod_scale, mod_gate,
        w_query, w_key, w_value, query_gain, key_gain, mix_lambda, context_lift, value_gain, w_out,
    ) = args
    R, D = latent.shape
    C = context.shape[0]
    head_width = query_gain.shape[0]
    cos, sin = rope_tables(R * n_sp * n_tp, head_width)
    QW, VWALL = w_query.shape[1], w_value.shape[1]
    heads = mix_lambda.shape[0]
    ROWS = R * n_tp
    HW = 2 * head_width
    KV = (QW + VWALL) // heads
    MC = mod_shift.shape[1]
    vm = pl.BlockSpec(memory_space=pltpu.VMEM)
    anywhere = pl.BlockSpec(memory_space=pl.ANY)
    smem = pl.BlockSpec(memory_space=pltpu.SMEM)
    dma = pltpu.SemaphoreType.DMA
    update = pl.pallas_call(
        functools.partial(kernel, n_sp, n_tp, n_dp, head_width),
        out_shape=pltpu.VMEM((R, D), F32),
        in_specs=[anywhere] * 14 + [smem, smem]
        + [anywhere] * 3,
        out_specs=vm,
        scratch_shapes=[
            pltpu.VMEM(cond.shape, BF),
            pltpu.VMEM(context_cond.shape, BF),
            pltpu.VMEM(norm_gain.shape, F32),
            pltpu.VMEM(query_gain.shape, F32),
            pltpu.VMEM(key_gain.shape, F32),
            pltpu.VMEM(value_gain.shape, F32),
            pltpu.VMEM((R, D), BF),
            pltpu.VMEM((4, R, D), BF),
            pltpu.VMEM((C, D), BF),
            pltpu.VMEM((3,) + mod_shift.shape, BF),
            pltpu.VMEM(w_query.shape, BF),
            pltpu.VMEM((2,) + w_key.shape, BF),
            pltpu.VMEM((4,) + w_out.shape, BF),
            pltpu.VMEM((2, ROWS, HW), F32),
            pltpu.VMEM((8, mod_shift.shape[0]), F32),
            pltpu.VMEM((8, MC), F32),
            pltpu.VMEM((n_sp - 1, 8, MC), F32),
            pltpu.VMEM((8, MC), F32),
            pltpu.VMEM((n_tp, 8, MC), F32),
            pltpu.VMEM((2, 8, D), F32),
            pltpu.VMEM((C + ROWS, D), BF),
            pltpu.VMEM((heads, ROWS, HW), BF),
            pltpu.VMEM((ROWS, HW), BF),
            pltpu.VMEM((2, 2 * ROWS, HW), BF),
            pltpu.VMEM((heads, C + ROWS, KV), BF),
            pltpu.VMEM((n_sp, ROWS, KV), BF),
            pltpu.VMEM((n_sp * C, KV), BF),
            pltpu.VMEM((2, 2 * ROWS, 2 * VWALL // heads), F32),
            pltpu.VMEM((8, R, VWALL // heads), BF),
            pltpu.VMEM((4, R, VWALL), BF),
            pltpu.VMEM((2 * QW, QW), BF),
            dma((13,)),
            dma(()), dma((4,)),
            dma(()), dma((6,)),
            dma(()), dma(()),
            dma(()), dma(()),
            dma(()), dma(()),
            dma(()), dma((n_sp,)),
            dma(()), dma(()),
            dma(()), dma(()),
            dma(()), dma((7,)),
            dma(()), dma((3,)),
            dma(()), dma((4,)),
        ],
        compiler_params=pltpu.CompilerParams(
            collective_id=0, has_side_effects=True, vmem_limit_bytes=66_100_000
        ),
        name="block",
    )(
        latent, context, cond, context_cond, norm_gain, mod_shift, mod_scale,
        mod_gate, w_query, w_key, w_value, query_gain, key_gain, value_gain, mix_lambda, context_lift, w_out,
        jnp.asarray(cos), jnp.asarray(sin),
    )
    return (latent.astype(F32) + update).astype(latent.dtype)


def solution(mesh):
    placed = (
        P(("dp", "sp", "tp"), None),
        P(("dp", "sp"), None),
        P(("dp", "sp")),
        P("sp"),
        P(),
        P("sp", "tp"),
        P("sp", "tp"),
        P("sp", "tp"),
        P(None, "tp"),
        P(None, "tp"),
        P(None, "tp"),
        P(),
        P(),
        P("tp"),
        P("tp"),
        P(),
        P("tp", None),
    )
    sizes = mesh.shape
    return jax.shard_map(
        functools.partial(on_device, sizes["sp"], sizes["tp"], sizes["dp"]),
        mesh=mesh,
        in_specs=placed,
        out_specs=P(("dp", "sp", "tp"), None),
        check_vma=False,
    )
```

time: 38.5 us -> 39.3 us (1.021)
  Pallas kernels: 37.5 us -> 38.3 us
    pallas_call x1, Pallas kernels: 37.5 us -> 38.3 us  [on_device(): pl.pallas_call(functools.partial(kernel, n_sp, n_tp, n_dp, head_width), o...]
where the time goes in v2:
time: 39.3 us; the launch traced here: 39.1 us
  Pallas kernels  38.3 us (97%)
  other arithmetic  0.75 us (2%)
    pallas_call x1, Pallas kernels, on_device(): pl.pallas_call(functools.partial(kernel, n_sp, n_tp, n_dp, head_width), o...  38.3 us

profile of v2, /device:TPU:0, one launch (start us, length us, event | category | flops | bytes accessed | tf_op | source)
XLA Modules:
  0.0 39.1 jit_solution(1071938084820806365)
XLA Ops:
  0.0 0.0 copy-start
  0.0 38.3 %block.1 = f32[64,2048]{1,0:T(8,128)S(1)} custom-call(bf16[64,2048]{1,0:T(8,128)(2,1)} %refs_0_.1, bf16[64,2048]{1,0:T(8,128)(2,1)} %refs_1_.1, bf16[512]{0:T(512)(128)(2,1)} %refs_2_.1, bf16[512]{0:T(512)(128)(2,1)} %refs_3_.1, f32[2048]{0:T(1024)} %refs_4_.1, bf16[512,512]{1,0:T(8,128)(2,1)} %refs_5_.1, bf16[512,512]{1,0:T(8,128)(2,1)} %refs_6_.1, ...), custom_call_target="tpu_custom_call" | custom-call | tf_op jit(solution)/shard_map/block/pallas_call | solution.py:544
  38.4 0.0 copy-done
  38.4 0.8 %add_convert_fusion = bf16[64,2048]{1,0:T(8,128)(2,1)} fusion(f32[64,2048]{1,0:T(8,128)S(1)} %block.1, bf16[64,2048]{1,0:T(8,128)(2,1)S(1)} %copy-done), kind=kLoop, calls=%fused_computation | loop fusion | flops 393216 | bytes 1048576 | tf_op jit(solution)/shard_map/convert_element_type | solution.py:604
Async XLA Ops:
  0.0 38.4 %copy-start = (bf16[64,2048]{1,0:T(8,128)(2,1)S(1)}, bf16[64,2048]{1,0:T(8,128)(2,1)}, u32[]{:S(2)}) copy-start(bf16[64,2048]{1,0:T(8,128)(2,1)} %refs_0_.1) | copy-start | bytes 786436

commit v3 on v2

--- a/solution.py
+++ b/solution.py
@@ -39,7 +39,7 @@
         act, part, mod_in, summed, mod_full, vecs, normed, qown, qin, qm, kvl, kvr, kvc, acc,
         mine, ho, grp,
         loc, s_swap, r_swap, s_lat, r_lat, s_mod, r_mod, s_mt, r_mt, s_vec, r_vec, s_kv, r_kv,
-        s_ctx, r_ctx, s_q, r_q, s_wo, r_wo, s_dd, r_dd, s_ho, r_ho,
+        s_ctx, r_ctx, s_q, r_q, s_wo, r_wo, s_wz, r_wz, s_dd, r_dd, s_ho, r_ho,
     ) = refs
     s = lax.axis_index("sp")
     t = lax.axis_index("tp")
@@ -61,6 +61,8 @@
     block = s + a * (s_opp - s)
     other_block = s_opp + a * (s - s_opp)
     d_work = d_ix - core + half
+    e = lax.rem(s, 2)
+    level = s + 1 - 2 * e
     R, D = own.shape
     PR = R // 4
     C = ctx.shape[0]
@@ -111,6 +113,7 @@
     acts = act[...].astype(BF)
     part[...] = jnp.zeros_like(part)
     drain(mw, loc.at[3])
+    l_wo = local(12, wo_h, wo.at[0])
     for j in range(3):
         res = jnp.dot(acts, mw[j], preferred_element_type=F32)
         part[2 * j : 2 * j + 2, :] = res[0:2]
@@ -144,6 +147,66 @@
         (along_x(j) if j < 2 else along_y(j)).wait_recv()
         onward(j).start()
 
+    HALF = wo.shape[1] // 2
+    QUART = HALF // 2
+    SH = QUART // 4
+
+    def wo_rows(at, count):
+        return pl.ds(pl.multiple_of(core * HALF + at, SH), count)
+
+    def wo_copy(i, src_slot, dst_slot, at, count, where):
+        rows = wo_rows(at, count)
+        return remote(wo.at[src_slot, rows], wo.at[dst_slot, rows], s_wo, r_wo.at[i], {"tp": where})
+
+    def wz_copy(k, q):
+        rows = wo_rows(q * QUART + (QUART - SH) * e, SH)
+        return remote(wo.at[k, rows], wo.at[k, rows], s_wz, r_wz.at[k - 1], {"sp": level})
+
+    def dd_copy(k, at, count):
+        rows = wo_rows(at, count)
+        return remote(wo.at[k, rows], wo.at[k, rows], s_dd, r_dd.at[k - 1], {"dp": partner})
+
+    def lead(i, src, dst, q, where):
+        return wo_copy(i, src, dst, q * QUART + (QUART - SH) * e, SH, where)
+
+    def rest(i, src, dst, q, where):
+        return wo_copy(i, src, dst, q * QUART + SH, QUART - 2 * SH, where)
+
+    lead_x = [lead(0, 0, 1, 0, nbr1), lead(2, 0, 1, 1, nbr1)]
+    lead_y = [lead(2, 0, 2, 0, nbr2), lead(1, 0, 2, 1, nbr2)]
+    lead_f = [lead(6, 1, 3, 0, nbr2), lead(6, 2, 3, 1, nbr1)]
+    rest_x = [rest(3, 0, 1, 0, nbr1), rest(5, 0, 1, 1, nbr1)]
+    rest_y = [rest(5, 0, 2, 0, nbr2), rest(4, 0, 2, 1, nbr2)]
+    rest_f = [rest(7, 1, 3, 0, nbr2), rest(8, 2, 3, 1, nbr1)]
+
+    def start(*copies):
+        for c in copies:
+            c.start()
+
+    def share_first():
+        lead_x[0].wait_recv()
+        wz_copy(1, 0).start()
+        lead_y[1].wait_recv()
+        wz_copy(2, 1).start()
+
+    def share_second():
+        drain(wo.at[1, pl.ds(0, 2 * SH)], r_wo.at[2])
+        wz_copy(1, 1).start()
+        wz_copy(2, 0).start()
+
+    def share_far():
+        wz_copy(3, 0).start()
+        wz_copy(3, 1).start()
+
+    def pass_rest():
+        rest_x[0].wait_recv()
+        rest_f[0].start()
+        rest_y[1].wait_recv()
+        rest_f[1].start()
+
+    near_leads = (lead_x[0], lead_y[1], lead_x[1], lead_y[0])
+    near_rests = (rest_x[0], rest_y[1], rest_x[1], rest_y[0])
+
     for k in range(1, n_sp):
         mod_copy(k).start()
 
@@ -155,8 +218,8 @@
 
     @pl.when(away)
     def _():
-        swap(0).start()
-        swap(1).start()
+        for j in range(4):
+            swap(j).start()
 
     l_ctx = local(4, ctx_h, ctx)
     local(5, wk_h, wkv.at[0])
@@ -169,7 +232,12 @@
         for j, (src, dst) in enumerate(((gain_h, gain_r), (qg_h, qg_r), (kg_h, kg_r), (vg_h, vg_r)))
     ]
     l_wq = local(11, wq_h, wq)
-    l_wo = local(12, wo_h, wo.at[0])
+
+    l_wo.wait()
+
+    @pl.when(away)
+    def _():
+        start(*near_leads)
 
     group = (
         lax.rem(lax.broadcasted_iota(jnp.int32, (2 * QW, QW), 0), QW) // head_width
@@ -198,51 +266,21 @@
     for k in range(1, 4):
         mt_copy(k).start()
 
-    HALF = wo.shape[1] // 2
-    QUART = HALF // 2
-    EIGHTH = QUART // 2
-
-    def wo_rows(at, count):
-        return pl.ds(pl.multiple_of(core * HALF + at, count), count)
-
-    def wo_copy(i, src_slot, dst_slot, at, count, where):
-        rows = wo_rows(at, count)
-        return remote(wo.at[src_slot, rows], wo.at[dst_slot, rows], s_wo, r_wo.at[i], {"tp": where})
-
-    def dd_copy(i, k, at, count):
-        rows = wo_rows(at, count)
-        return remote(wo.at[k, rows], wo.at[k, rows], s_dd, r_dd.at[i], {"dp": partner})
-
-    wx0 = wo_copy(0, 0, 1, 0, QUART, nbr1)
-    wy1 = wo_copy(1, 0, 2, QUART, QUART, nbr2)
-    wx1 = wo_copy(2, 0, 1, QUART, QUART, nbr1)
-    wy0 = wo_copy(2, 0, 2, 0, QUART, nbr2)
-    wf = [
-        wo_copy(3, 1, 3, 0, EIGHTH, nbr2),
-        wo_copy(4, 1, 3, EIGHTH, EIGHTH, nbr2),
-        wo_copy(5, 2, 3, QUART, EIGHTH, nbr1),
-        wo_copy(6, 2, 3, QUART + EIGHTH, EIGHTH, nbr1),
-    ]
-    dd = [dd_copy(0, 1, 0, HALF), dd_copy(1, 2, 0, HALF)] + [
-        dd_copy(2, 3, i * EIGHTH, EIGHTH) for i in range(4)
-    ]
-    l_wo.wait()
-
     @pl.when(home)
     def _():
         for j in (0, 2, 1, 3):
             pass_on(j)
-        for c in (wx0, wy1, wx1, wy0):
-            c.start()
-
-    @pl.when(away)
-    def _():
-        swap(2).start()
-        swap(3).start()
+        start(*near_leads)
+
+    @pl.when(away)
+    def _():
         for j in range(4):
             swap(j).wait_recv()
             along_x(j).start()
             along_y(j).start()
+            if j == 1:
+                share_first()
+                share_second()
         pass_on(0)
         pass_on(1)
 
@@ -262,11 +300,7 @@
     def _():
         vec_copy.start()
 
-    @pl.when(away)
-    def _():
-        vec_copy.wait_recv()
-
-    def norm_rows(src, row, count, dst_at):
+    def norm_rows(src, row, count, dst_at, slot):
         step = 16
 
         @pl.loop(0, count // step, unroll=True)
@@ -275,7 +309,7 @@
             v = src[pl.ds(at, step), :].astype(F32)
             inv = lax.rsqrt(jnp.mean(v * v, axis=-1, keepdims=True) + token_eps)
             normed[pl.ds(dst_at + at, step), :] = (
-                v * inv * vecs[a, 2 + row : 3 + row, :] + vecs[a, row : row + 1, :]
+                v * inv * vecs[slot, 2 + row : 3 + row, :] + vecs[slot, row : row + 1, :]
             ).astype(BF)
 
     def head_norm(x):
@@ -314,12 +348,12 @@
         for h in range(n_head):
             kvl[h, first : first + count, HW:] = vv[:, h * VW : (h + 1) * VW]
 
-    def project_queries():
-        x = normed[C:, :]
+    def project_queries(first, last):
+        x = normed[C + first * R : C + last * R, :]
         qq = head_norm(jnp.dot(x, wq[...], preferred_element_type=F32))
-        for k in range(4):
+        for k in range(first, last):
             for h in range(n_head):
-                y = qq[k * R : (k + 1) * R, h * HW : (h + 1) * HW] * q_gain
+                y = qq[(k - first) * R : (k - first + 1) * R, h * HW : (h + 1) * HW] * q_gain
                 qown[h, k * R : (k + 1) * R, :] = (
                     turn(y, *turns_of(k)) * (head_width ** -0.5)
                 ).astype(BF)
@@ -362,33 +396,45 @@
                     ctx_copy(lax.rem(s_opp + j, H) + H - base, head).start()
 
     l_ctx.wait()
-    norm_rows(ctx, 1, C, 0)
-    norm_rows(lat.at[0], 0, R, C)
+    norm_rows(ctx, 1, C, 0, 0)
     drain(wkv, loc.at[5])
     drain(turns, loc.at[6])
-    project(0, C + R, C)
-    send_block(0, R)
-    send_ctx()
-
-    @pl.when(away)
-    def _():
+
+    @pl.when(home)
+    def _():
+        norm_rows(lat.at[0], 0, R, C, 0)
+        project(0, C + R, C)
+        send_block(0, R)
+        send_ctx()
+        drain(lat.at[1], r_lat.at[4])
+        norm_rows(lat.at[1], 0, R, C + R, 0)
+        norm_rows(lat.at[2], 0, R, C + 2 * R, 0)
+        project(C + R, 2 * R, 0)
+        send_block(R, 2 * R)
+
+    @pl.when(away)
+    def _():
+        project(0, C, C)
+        send_ctx()
         pass_on(2)
         pass_on(3)
-        for c in (wx0, wy1, wx1, wy0):
-            c.start()
-
-    drain(lat.at[1], r_lat.at[4])
-    norm_rows(lat.at[1], 0, R, C + R)
-    norm_rows(lat.at[2], 0, R, C + 2 * R)
-    project(C + R, 2 * R, 0)
-    send_block(R, 2 * R)
+        start(*lead_f, *near_rests)
+        vec_copy.wait_recv()
+        norm_rows(lat.at[0], 0, R, C, 1)
+        drain(lat.at[1], r_lat.at[4])
+        norm_rows(lat.at[1], 0, R, C + R, 1)
+        norm_rows(lat.at[2], 0, R, C + 2 * R, 1)
+        project(C, 3 * R, 0)
+        send_block(0, 3 * R)
+
+    l_wq.wait()
+    project_queries(0, 3)
     drain(lat.at[3], r_lat.at[5])
-    norm_rows(lat.at[3], 0, R, C + 3 * R)
+    norm_rows(lat.at[3], 0, R, C + 3 * R, a)
     project(C + 3 * R, R, 0)
     send_block(3 * R, R)
 
-    l_wq.wait()
-    project_queries()
+    project_queries(3, 4)
     q_copy = remote(qown.at[1 - core], qin, s_q, r_q, {"dp": partner})
     q_copy.start()
     split_maps(qown[core], 0)
@@ -415,17 +461,38 @@
                 else:
                     acc[m, rows, :] += add
 
+    @pl.when(home)
+    def _():
+        share_first()
+        start(*lead_f)
+
+    @pl.when(jnp.logical_and(home, core == 0))
+    def _():
+        start(*near_rests)
+
     attend(kvl.at[core], C, ROWS, 0, ROWS, True, None)
-    wx0.wait_recv()
-    wf[0].start()
-    wf[1].start()
-    wy1.wait_recv()
-    wf[2].start()
-    wf[3].start()
+
+    @pl.when(jnp.logical_and(home, core == 1))
+    def _():
+        drain(wo.at[3, pl.ds(0, 2 * SH)], r_wo.at[6])
+        start(*near_rests)
+
     q_copy.wait_recv()
     split_maps(qin[...], ROWS)
     attend(kvl.at[core], C, ROWS, ROWS, ROWS, True, None)
 
+    pass_rest()
+
+    @pl.when(home)
+    def _():
+        share_second()
+
+    @pl.when(jnp.logical_or(away, core == 0))
+    def _():
+        drain(wo.at[3, pl.ds(0, 2 * SH)], r_wo.at[6])
+
+    share_far()
+
     def attend_block(slot, i):
         drain(kvr.at[slot], r_kv.at[i])
         attend(kvr.at[slot], 0, ROWS, 0, 2 * ROWS, False, None)
@@ -443,60 +510,61 @@
 
     attend(kvc, 0, n_sp * C, 0, 2 * ROWS, False, lift)
     attend_block(other_block, 1 - a)
-    drain(wo.at[1, pl.ds(0, HALF)], r_wo.at[2])
-    dd[0].start()
-    dd[1].start()
     for j in range(1, H):
         attend_block(lax.rem(base + lax.rem(s - base + H - j, H) + H, n_sp), 2 * j + 1)
 
     def ho_copy(q, k):
-        lanes = pl.ds(pl.multiple_of(core * VW, VW), VW)
-        return remote(mine.at[4 * q + k], ho.at[k, :, lanes], s_ho, r_ho.at[k],
-                      {"dp": d_work, "sp": other_block if q else block, "tp": peers[k]})
-
-    for q, k in ((1, 3), (0, 3), (1, 1), (0, 1), (1, 2), (0, 2), (1, 0), (0, 0)):
-        rows = slice((4 * q + k) * R, (4 * q + k + 1) * R)
+        lanes = pl.ds(pl.multiple_of(k * n_head * VW + core * VW, VW), VW)
+        return remote(mine.at[q, pl.ds(k * R, R)], ho.at[:, lanes], s_ho, r_ho.at[k],
+                      {"dp": d_work, "sp": block + q * (other_block - block), "tp": peers[k]})
+
+    for q in (1 - a, a):
+        rows = pl.ds(pl.multiple_of(q * ROWS, ROWS), ROWS)
         a0 = acc[0, rows, :]
         a1 = acc[1, rows, :]
         mixed = a0[:, :VW] / a0[:, VW:] - lam_r[core] * (a1[:, :VW] / a1[:, VW:])
         inv = lax.rsqrt(jnp.mean(mixed * mixed, axis=-1, keepdims=True) + head_eps)
-        value = (mixed * inv * v_gain * head_factor).astype(BF)
-        mine[4 * q + k, :, :] = value
-        if q or k:
+        mine[q, :, :] = (mixed * inv * v_gain * head_factor).astype(BF)
+        for k in (3, 1, 2):
             ho_copy(q, k).start()
-        else:
-            @pl.when(away)
-            def _():
-                ho_copy(0, 0).start()
-
-            for h in range(2):
-                @pl.when(jnp.logical_and(home, core == h))
-                def _():
-                    ho[0, :, h * VW : (h + 1) * VW] = value
-
-    for i in range(4):
-        wf[i].wait_recv()
-        dd[2 + i].start()
-
-    @pl.when(home)
-    def _():
-        drain(mine.at[0], r_ho.at[0])
-
-    @pl.when(away)
-    def _():
-        drain(ho.at[0], r_ho.at[0])
-
-    for k in range(4):
-        if k:
-            drain(wo.at[k, pl.ds(0, HALF)], r_dd.at[k - 1])
-            drain(ho.at[k], r_ho.at[k])
-        add = jnp.dot(ho[k], wo[k], preferred_element_type=F32)
-        if k == 0:
-            out_r[...] = add
-        elif k < 3:
-            out_r[...] += add
-        else:
-            out_r[...] = vecs[0, 4:5, :] * (out_r[...] + add)
+        if q is not a:
+            ho_copy(q, 0).start()
+
+    @pl.when(away)
+    def _():
+        ho_copy(a, 0).start()
+
+    for h in range(2):
+        @pl.when(jnp.logical_and(home, core == h))
+        def _():
+            ho[:, h * VW : (h + 1) * VW] = mine[0, 0:R, :]
+
+    drain(wo.at[1, pl.ds(0, 2 * (QUART - 2 * SH))], r_wo.at[5])
+    for k in range(1, 3):
+        drain(wo.at[k, pl.ds(0, 2 * SH)], r_wz.at[k - 1])
+        dd_copy(k, 0, HALF).start()
+    drain(wo.at[3, pl.ds(0, 2 * SH)], r_wz.at[2])
+    for q in range(2):
+        dd_copy(3, q * QUART, SH).start()
+        dd_copy(3, (q + 1) * QUART - SH, SH).start()
+    for q in range(2):
+        rest_f[q].wait_recv()
+        dd_copy(3, q * QUART + SH, QUART - 2 * SH).start()
+
+    for k in range(1, 4):
+        drain(wo.at[k, pl.ds(0, HALF)], r_dd.at[k - 1])
+        drain(mine.at[0, pl.ds(0, 2 * R)], r_ho.at[k])
+
+    @pl.when(home)
+    def _():
+        drain(mine.at[0, pl.ds(0, R)], r_ho.at[0])
+
+    @pl.when(away)
+    def _():
+        drain(mine.at[0, pl.ds(0, 2 * R)], r_ho.at[0])
+
+    weights = wo[...].reshape(-1, D)
+    out_r[...] = vecs[0, 4:5, :] * jnp.dot(ho[...], weights, preferred_element_type=F32)
 
     def sent(ref, sem):
         remote(ref, ref, sem, sem, {"dp": partner}).wait_send()
@@ -505,7 +573,8 @@
     sent(mod_full.at[0:3], s_mt)
     sent(lat.at[0:3], s_lat)
     sent(kvr.at[0 : n_sp - 1], s_kv)
-    sent(wo.at[0:3, pl.ds(0, HALF)], s_wo)
+    sent(wo.at[0:3, pl.ds(0, 2 * (QUART - SH))], s_wo)
+    sent(wo.at[0:3, pl.ds(0, 2 * SH)], s_wz)
     sent(wo.at[0:3, pl.ds(0, HALF)], s_dd)
     q_copy.wait_send()
 
@@ -513,7 +582,7 @@
     def _():
         vec_copy.wait_send()
         sent(kvc.at[pl.ds(0, (n_sp - 1) * C)], s_ctx)
-        sent(mine.at[1:8], s_ho)
+        sent(qm.at[0, pl.ds(0, 7 * R)], s_ho)
 
     @pl.when(away)
     def _():
@@ -576,8 +645,8 @@
             pltpu.VMEM((n_sp, ROWS, KV), BF),
             pltpu.VMEM((n_sp * C, KV), BF),
             pltpu.VMEM((2, 2 * ROWS, 2 * VWALL // heads), F32),
-            pltpu.VMEM((8, R, VWALL // heads), BF),
-            pltpu.VMEM((4, R, VWALL), BF),
+            pltpu.VMEM((2, ROWS, VWALL // heads), BF),
+            pltpu.VMEM((R, n_tp * VWALL), BF),
             pltpu.VMEM((2 * QW, QW), BF),
             dma((13,)),
             dma(()), dma((4,)),
@@ -588,7 +657,8 @@
             dma(()), dma((n_sp,)),
             dma(()), dma(()),
             dma(()), dma(()),
-            dma(()), dma((7,)),
+            dma(()), dma((9,)),
+            dma(()), dma((3,)),
             dma(()), dma((3,)),
             dma(()), dma((4,)),
         ],

time: 39.3 us -> 37.1 us (0.944)
  the two profiles are of different devices: /device:TPU:0 before, /device:TPU:1 now
where the time goes in v3:
time: 37.1 us; the launch traced here: 36.9 us
  Pallas kernels  36.2 us (98%)
  other arithmetic  0.75 us (2%)
    pallas_call x1, Pallas kernels, on_device(): pl.pallas_call(functools.partial(kernel, n_sp, n_tp, n_dp, head_width), o...  36.2 us
    convert_element_type x1, other arithmetic, on_device(): return (latent.astype(F32) + update).astype(latent.dtype)  0.75 us

profile of v3, /device:TPU:1, one launch (start us, length us, event | category | flops | bytes accessed | tf_op | source)
XLA Modules:
  0.0 36.9 jit_solution(17055975784360854104)
XLA Ops:
  0.0 0.0 copy-start
  0.0 36.2 %block.1 = f32[64,2048]{1,0:T(8,128)S(1)} custom-call(bf16[64,2048]{1,0:T(8,128)(2,1)} %refs_0_.1, bf16[64,2048]{1,0:T(8,128)(2,1)} %refs_1_.1, bf16[512]{0:T(512)(128)(2,1)} %refs_2_.1, bf16[512]{0:T(512)(128)(2,1)} %refs_3_.1, f32[2048]{0:T(1024)} %refs_4_.1, bf16[512,512]{1,0:T(8,128)(2,1)} %refs_5_.1, bf16[512,512]{1,0:T(8,128)(2,1)} %refs_6_.1, ...), custom_call_target="tpu_custom_call" | custom-call | tf_op jit(solution)/shard_map/block/pallas_call | solution.py:613
  36.2 0.0 copy-done
  36.2 0.8 %add_convert_fusion = bf16[64,2048]{1,0:T(8,128)(2,1)} fusion(f32[64,2048]{1,0:T(8,128)S(1)} %block.1, bf16[64,2048]{1,0:T(8,128)(2,1)S(1)} %copy-done), kind=kLoop, calls=%fused_computation | loop fusion | flops 393216 | bytes 1048576 | tf_op jit(solution)/shard_map/convert_element_type | solution.py:674
Async XLA Ops:
  0.0 36.2 %copy-start = (bf16[64,2048]{1,0:T(8,128)(2,1)S(1)}, bf16[64,2048]{1,0:T(8,128)(2,1)}, u32[]{:S(2)}) copy-start(bf16[64,2048]{1,0:T(8,128)(2,1)} %refs_0_.1) | copy-start | bytes 786436

commit v4 on v3

--- a/solution.py
+++ b/solution.py
@@ -270,6 +270,9 @@
     def _():
         for j in (0, 2, 1, 3):
             pass_on(j)
+
+    @pl.when(jnp.logical_and(home, core == 1))
+    def _():
         start(*near_leads)
 
     @pl.when(away)
@@ -412,6 +415,10 @@
         project(C + R, 2 * R, 0)
         send_block(R, 2 * R)
 
+    @pl.when(jnp.logical_and(home, core == 0))
+    def _():
+        start(*near_leads)
+
     @pl.when(away)
     def _():
         project(0, C, C)
@@ -439,7 +446,7 @@
     q_copy.start()
     split_maps(qown[core], 0)
 
-    QB = 2 * R
+    QB = 4 * R
     lift = lift_r[core]
 
     def attend(block, at, keys, start_row, count, first, plus):
@@ -481,11 +488,11 @@
     split_maps(qin[...], ROWS)
     attend(kvl.at[core], C, ROWS, ROWS, ROWS, True, None)
 
+    @pl.when(home)
+    def _():
+        share_second()
+
     pass_rest()
-
-    @pl.when(home)
-    def _():
-        share_second()
 
     @pl.when(jnp.logical_or(away, core == 0))
     def _():
@@ -564,7 +571,15 @@
         drain(mine.at[0, pl.ds(0, 2 * R)], r_ho.at[0])
 
     weights = wo[...].reshape(-1, D)
-    out_r[...] = vecs[0, 4:5, :] * jnp.dot(ho[...], weights, preferred_element_type=F32)
+    mixture = vecs[0, 4:5, :] * jnp.dot(ho[...], weights, preferred_element_type=F32)
+
+    @pl.when(home)
+    def _():
+        out_r[...] = (lat[0].astype(F32) + mixture).astype(BF)
+
+    @pl.when(away)
+    def _():
+        out_r[...] = (own[...].astype(F32) + mixture).astype(BF)
 
     def sent(ref, sem):
         remote(ref, ref, sem, sem, {"dp": partner}).wait_send()
@@ -612,7 +627,7 @@
     dma = pltpu.SemaphoreType.DMA
     update = pl.pallas_call(
         functools.partial(kernel, n_sp, n_tp, n_dp, head_width),
-        out_shape=pltpu.VMEM((R, D), F32),
+        out_shape=pltpu.VMEM((R, D), BF),
         in_specs=[anywhere] * 14 + [smem, smem]
         + [anywhere] * 3,
         out_specs=vm,
@@ -671,7 +686,7 @@
         mod_gate, w_query, w_key, w_value, query_gain, key_gain, value_gain, mix_lambda, context_lift, w_out,
         jnp.asarray(cos), jnp.asarray(sin),
     )
-    return (latent.astype(F32) + update).astype(latent.dtype)
+    return update
 
 
 def solution(mesh):

time: 37.1 us -> 35.2 us (0.949)
  the two profiles are of different devices: /device:TPU:1 before, /device:TPU:0 now
where the time goes in v4:
time: 35.2 us; the launch traced here: 35 us
  Pallas kernels  34.3 us (97%)
  local copies, waits for them, and re-layouts  0.71 us (2%)
    pallas_call x1, Pallas kernels, on_device(): pl.pallas_call(functools.partial(kernel, n_sp, n_tp, n_dp, head_width), o...  34.3 us
    unnamed x1, local copies, waits for them, and re-layouts  0.71 us

profile of v4, /device:TPU:0, one launch (start us, length us, event | category | flops | bytes accessed | tf_op | source)
XLA Modules:
  0.0 35.0 jit_solution(13231134262590451259)
XLA Ops:
  0.0 34.3 %block.1 = bf16[64,2048]{1,0:T(8,128)(2,1)S(1)} custom-call(bf16[64,2048]{1,0:T(8,128)(2,1)} %refs_0_.1, bf16[64,2048]{1,0:T(8,128)(2,1)} %refs_1_.1, bf16[512]{0:T(512)(128)(2,1)} %refs_2_.1, bf16[512]{0:T(512)(128)(2,1)} %refs_3_.1, f32[2048]{0:T(1024)} %refs_4_.1, bf16[512,512]{1,0:T(8,128)(2,1)} %refs_5_.1, bf16[512,512]{1,0:T(8,128)(2,1)} %refs_6_.1, ...), custom_call_target="tpu_custom_call" | custom-call | tf_op jit(solution)/shard_map/block/pallas_call | solution.py:628
  34.3 0.7 %copy.21 = bf16[64,2048]{1,0:T(8,128)(2,1)} copy(bf16[64,2048]{1,0:T(8,128)(2,1)S(1)} %block.1) | data formatting | bytes 524288

commit v5 on v4

--- a/solution.py
+++ b/solution.py
@@ -37,7 +37,7 @@
         cond_r, cctx_r, gain_r, qg_r, kg_r, vg_r,
         own, lat, ctx, mw, wq, wkv, wo, turns,
         act, part, mod_in, summed, mod_full, vecs, normed, qown, qin, qm, kvl, kvr, kvc, acc,
-        mine, ho, grp,
+        mine, ho, grp, partial,
         loc, s_swap, r_swap, s_lat, r_lat, s_mod, r_mod, s_mt, r_mt, s_vec, r_vec, s_kv, r_kv,
         s_ctx, r_ctx, s_q, r_q, s_wo, r_wo, s_wz, r_wz, s_dd, r_dd, s_ho, r_ho,
     ) = refs
@@ -277,31 +277,42 @@
 
     @pl.when(away)
     def _():
+        @pl.when(core == 1)
+        def _():
+            share_first()
+            share_second()
+
         for j in range(4):
             swap(j).wait_recv()
+            along_y(j).start()
             along_x(j).start()
-            along_y(j).start()
-            if j == 1:
-                share_first()
-                share_second()
+            if j == 3:
+                @pl.when(core == 0)
+                def _():
+                    share_first()
+                    share_second()
+
         pass_on(0)
         pass_on(1)
 
-    drain(mod_full.at[0:3], r_mt)
-
     def full_row(j):
         return jnp.concatenate([mod_full[q, j : j + 1, :] for q in range(n_tp)], axis=1)
 
-    vecs[0, 0:1, :] = full_row(0)
-    vecs[0, 1:2, :] = full_row(1)
-    vecs[0, 2:3, :] = gain * (1.0 + full_row(2))
-    vecs[0, 3:4, :] = gain * (1.0 + full_row(3))
-    vecs[0, 4:8, :] = jnp.broadcast_to(full_row(4), (4, D))
     vec_copy = remote(vecs.at[0], vecs.at[1], s_vec, r_vec, {"dp": partner})
 
     @pl.when(home)
     def _():
+        drain(mod_full.at[0:3], r_mt)
+        vecs[0, 0:1, :] = full_row(0)
+        vecs[0, 1:2, :] = full_row(1)
+        vecs[0, 2:3, :] = gain * (1.0 + full_row(2))
+        vecs[0, 3:4, :] = gain * (1.0 + full_row(3))
+        vecs[0, 4:8, :] = jnp.broadcast_to(full_row(4), (4, D))
         vec_copy.start()
+
+    @pl.when(away)
+    def _():
+        vec_copy.wait_recv()
 
     def norm_rows(src, row, count, dst_at, slot):
         step = 16
@@ -399,7 +410,7 @@
                     ctx_copy(lax.rem(s_opp + j, H) + H - base, head).start()
 
     l_ctx.wait()
-    norm_rows(ctx, 1, C, 0, 0)
+    norm_rows(ctx, 1, C, 0, a)
     drain(wkv, loc.at[5])
     drain(turns, loc.at[6])
 
@@ -426,7 +437,6 @@
         pass_on(2)
         pass_on(3)
         start(*lead_f, *near_rests)
-        vec_copy.wait_recv()
         norm_rows(lat.at[0], 0, R, C, 1)
         drain(lat.at[1], r_lat.at[4])
         norm_rows(lat.at[1], 0, R, C + R, 1)
@@ -520,6 +530,10 @@
     for j in range(1, H):
         attend_block(lax.rem(base + lax.rem(s - base + H - j, H) + H, n_sp), 2 * j + 1)
 
+    @pl.when(away)
+    def _():
+        drain(mod_full.at[0:3], r_mt)
+
     def ho_copy(q, k):
         lanes = pl.ds(pl.multiple_of(k * n_head * VW + core * VW, VW), VW)
         return remote(mine.at[q, pl.ds(k * R, R)], ho.at[:, lanes], s_ho, r_ho.at[k],
@@ -532,7 +546,7 @@
         mixed = a0[:, :VW] / a0[:, VW:] - lam_r[core] * (a1[:, :VW] / a1[:, VW:])
         inv = lax.rsqrt(jnp.mean(mixed * mixed, axis=-1, keepdims=True) + head_eps)
         mine[q, :, :] = (mixed * inv * v_gain * head_factor).astype(BF)
-        for k in (3, 1, 2):
+        for k in (3, 2, 1):
             ho_copy(q, k).start()
         if q is not a:
             ho_copy(q, 0).start()
@@ -558,10 +572,23 @@
         rest_f[q].wait_recv()
         dd_copy(3, q * QUART + SH, QUART - 2 * SH).start()
 
-    for k in range(1, 4):
+    def arrived(k):
         drain(wo.at[k, pl.ds(0, HALF)], r_dd.at[k - 1])
         drain(mine.at[0, pl.ds(0, 2 * R)], r_ho.at[k])
 
+    KW = n_head * VW
+
+    @pl.when(away)
+    def _():
+        vecs[0, 4:8, :] = jnp.broadcast_to(full_row(4), (4, D))
+
+    arrived(1)
+    arrived(2)
+    partial[...] = jnp.dot(
+        ho[:, KW : 3 * KW], wo[1:3].reshape(-1, D), preferred_element_type=F32
+    )
+    arrived(3)
+
     @pl.when(home)
     def _():
         drain(mine.at[0, pl.ds(0, R)], r_ho.at[0])
@@ -570,8 +597,9 @@
     def _():
         drain(mine.at[0, pl.ds(0, 2 * R)], r_ho.at[0])
 
-    weights = wo[...].reshape(-1, D)
-    mixture = vecs[0, 4:5, :] * jnp.dot(ho[...], weights, preferred_element_type=F32)
+    late = jnp.dot(ho[:, 0:KW], wo[0], preferred_element_type=F32)
+    late += jnp.dot(ho[:, 3 * KW :], wo[3], preferred_element_type=F32)
+    mixture = vecs[0, 4:5, :] * (partial[...] + late)
 
     @pl.when(home)
     def _():
@@ -663,6 +691,7 @@
             pltpu.VMEM((2, ROWS, VWALL // heads), BF),
             pltpu.VMEM((R, n_tp * VWALL), BF),
             pltpu.VMEM((2 * QW, QW), BF),
+            pltpu.VMEM((R, D), F32),
             dma((13,)),
             dma(()), dma((4,)),
             dma(()), dma((6,)),

time: 35.2 us -> 34.7 us (0.986)
  Pallas kernels: 34.3 us -> 33.6 us
    pallas_call x1, Pallas kernels: 34.3 us -> 33.6 us  [on_device(): pl.pallas_call(functools.partial(kernel, n_sp, n_tp, n_dp, head_width), o...]
where the time goes in v5:
time: 34.7 us; the launch traced here: 34.3 us
  Pallas kernels  33.6 us (97%)
  local copies, waits for them, and re-layouts  0.71 us (2%)
    pallas_call x1, Pallas kernels, on_device(): pl.pallas_call(functools.partial(kernel, n_sp, n_tp, n_dp, head_width), o...  33.6 us
    unnamed x1, local copies, waits for them, and re-layouts  0.71 us

profile of v5, /device:TPU:0, one launch (start us, length us, event | category | flops | bytes accessed | tf_op | source)
XLA Modules:
  0.0 34.3 jit_solution(14781685333786135880)
XLA Ops:
  0.0 33.6 %block.1 = bf16[64,2048]{1,0:T(8,128)(2,1)S(1)} custom-call(bf16[64,2048]{1,0:T(8,128)(2,1)} %refs_0_.1, bf16[64,2048]{1,0:T(8,128)(2,1)} %refs_1_.1, bf16[512]{0:T(512)(128)(2,1)} %refs_2_.1, bf16[512]{0:T(512)(128)(2,1)} %refs_3_.1, f32[2048]{0:T(1024)} %refs_4_.1, bf16[512,512]{1,0:T(8,128)(2,1)} %refs_5_.1, bf16[512,512]{1,0:T(8,128)(2,1)} %refs_6_.1, ...), custom_call_target="tpu_custom_call" | custom-call | tf_op jit(solution)/shard_map/block/pallas_call | solution.py:656
  33.6 0.7 %copy.21 = bf16[64,2048]{1,0:T(8,128)(2,1)} copy(bf16[64,2048]{1,0:T(8,128)(2,1)S(1)} %block.1) | data formatting | bytes 524288

commit v6 on v5

--- a/solution.py
+++ b/solution.py
@@ -105,18 +105,16 @@
     for j, h in enumerate((ms_h, msc_h, mg_h)):
         local(3, h, mw.at[j])
 
-    act[...] = jnp.zeros_like(act)
+    rows = []
     for row, ref in ((0, cond_r), (1, cctx_r)):
         l_one[row].wait()
         v = ref[...].astype(F32).reshape(1, -1)
-        act[row : row + 1, :] = v / (1.0 + jnp.exp(-v))
-    acts = act[...].astype(BF)
-    part[...] = jnp.zeros_like(part)
+        rows.append(v / (1.0 + jnp.exp(-v)))
+    acts = jnp.concatenate(rows + [jnp.zeros((6, rows[0].shape[1]), F32)], axis=0).astype(BF)
     drain(mw, loc.at[3])
     l_wo = local(12, wo_h, wo.at[0])
-    for j in range(3):
-        res = jnp.dot(acts, mw[j], preferred_element_type=F32)
-        part[2 * j : 2 * j + 2, :] = res[0:2]
+    res = [jnp.dot(acts, mw[j], preferred_element_type=F32) for j in range(3)]
+    part[...] = jnp.concatenate([r[0:2] for r in res] + [res[2][6:8]], axis=0)
 
     drain(own, loc.at[0])
     pl.semaphore_wait(bar, len(greeted))
@@ -564,13 +562,14 @@
     for k in range(1, 3):
         drain(wo.at[k, pl.ds(0, 2 * SH)], r_wz.at[k - 1])
         dd_copy(k, 0, HALF).start()
-    drain(wo.at[3, pl.ds(0, 2 * SH)], r_wz.at[2])
     for q in range(2):
-        dd_copy(3, q * QUART, SH).start()
-        dd_copy(3, (q + 1) * QUART - SH, SH).start()
+        dd_copy(3, q * QUART + (QUART - SH) * e, SH).start()
     for q in range(2):
         rest_f[q].wait_recv()
         dd_copy(3, q * QUART + SH, QUART - 2 * SH).start()
+    drain(wo.at[3, pl.ds(0, 2 * SH)], r_wz.at[2])
+    for q in range(2):
+        dd_copy(3, q * QUART + (QUART - SH) * (1 - e), SH).start()
 
     def arrived(k):
         drain(wo.at[k, pl.ds(0, HALF)], r_dd.at[k - 1])

time: 34.7 us -> 34.6 us (level)
  no operation moved by 1% of the time
where the time goes in v6:
time: 34.6 us; the launch traced here: 34.3 us
  Pallas kernels  33.6 us (97%)
  local copies, waits for them, and re-layouts  0.71 us (2%)
    pallas_call x1, Pallas kernels, on_device(): pl.pallas_call(functools.partial(kernel, n_sp, n_tp, n_dp, head_width), o...  33.6 us
    unnamed x1, local copies, waits for them, and re-layouts  0.71 us

profile of v6, /device:TPU:0, one launch (start us, length us, event | category | flops | bytes accessed | tf_op | source)
XLA Modules:
  0.0 34.3 jit_solution(144831924097689640)
XLA Ops:
  0.0 33.6 %block.1 = bf16[64,2048]{1,0:T(8,128)(2,1)S(1)} custom-call(bf16[64,2048]{1,0:T(8,128)(2,1)} %refs_0_.1, bf16[64,2048]{1,0:T(8,128)(2,1)} %refs_1_.1, bf16[512]{0:T(512)(128)(2,1)} %refs_2_.1, bf16[512]{0:T(512)(128)(2,1)} %refs_3_.1, f32[2048]{0:T(1024)} %refs_4_.1, bf16[512,512]{1,0:T(8,128)(2,1)} %refs_5_.1, bf16[512,512]{1,0:T(8,128)(2,1)} %refs_6_.1, ...), custom_call_target="tpu_custom_call" | custom-call | tf_op jit(solution)/shard_map/block/pallas_call | solution.py:655
  33.6 0.7 %copy.21 = bf16[64,2048]{1,0:T(8,128)(2,1)} copy(bf16[64,2048]{1,0:T(8,128)(2,1)S(1)} %block.1) | data formatting | bytes 524288

commit v7 on v6

--- a/solution.py
+++ b/solution.py
@@ -449,6 +449,11 @@
     project(C + 3 * R, R, 0)
     send_block(3 * R, R)
 
+    @pl.when(jnp.logical_and(home, core == 0))
+    def _():
+        start(rest_x[0], rest_y[1])
+
+
     project_queries(3, 4)
     q_copy = remote(qown.at[1 - core], qin, s_q, r_q, {"dp": partner})
     q_copy.start()
@@ -483,7 +488,7 @@
 
     @pl.when(jnp.logical_and(home, core == 0))
     def _():
-        start(*near_rests)
+        start(rest_x[1], rest_y[0])
 
     attend(kvl.at[core], C, ROWS, 0, ROWS, True, None)
 

time: 34.6 us -> 34.6 us (level)
  no operation moved by 1% of the time
where the time goes in v7:
time: 34.6 us; the launch traced here: 34.4 us
  Pallas kernels  33.7 us (97%)
  local copies, waits for them, and re-layouts  0.71 us (2%)
    pallas_call x1, Pallas kernels, on_device(): pl.pallas_call(functools.partial(kernel, n_sp, n_tp, n_dp, head_width), o...  33.7 us
    unnamed x1, local copies, waits for them, and re-layouts  0.71 us

profile of v7, /device:TPU:0, one launch (start us, length us, event | category | flops | bytes accessed | tf_op | source)
XLA Modules:
  0.0 34.4 jit_solution(9786140200887553673)
XLA Ops:
  0.0 33.7 %block.1 = bf16[64,2048]{1,0:T(8,128)(2,1)S(1)} custom-call(bf16[64,2048]{1,0:T(8,128)(2,1)} %refs_0_.1, bf16[64,2048]{1,0:T(8,128)(2,1)} %refs_1_.1, bf16[512]{0:T(512)(128)(2,1)} %refs_2_.1, bf16[512]{0:T(512)(128)(2,1)} %refs_3_.1, f32[2048]{0:T(1024)} %refs_4_.1, bf16[512,512]{1,0:T(8,128)(2,1)} %refs_5_.1, bf16[512,512]{1,0:T(8,128)(2,1)} %refs_6_.1, ...), custom_call_target="tpu_custom_call" | custom-call | tf_op jit(solution)/shard_map/block/pallas_call | solution.py:660
  33.7 0.7 %copy.21 = bf16[64,2048]{1,0:T(8,128)(2,1)} copy(bf16[64,2048]{1,0:T(8,128)(2,1)S(1)} %block.1) | data formatting | bytes 524288
